TPU v7x, 256 devices: a whole 4x4x8 slice. The times are simulated.
256 devices in a mesh: rep: 2 (over z_hi), fs: 16 (over z_lo, x), tp: 8 (over y, core).
Axes of the slice: x: 4, y: 4, z: 8 (z_hi: 2, z_lo: 4; z = z_hi * 4 + z_lo), core: 2. Of those that a mesh axis runs over, the one named last changes fastest.
Arguments:
- tokens: bfloat16 [24576, 2048], P(('rep', 'fs'), 'tp'), may hold values from -6 to 6
- gain_mix: bfloat16 [2048], replicated, may hold values from 0.099609375 to 1.8984375
- query_weight: bfloat16 [2048, 1024], P('fs', 'tp'), may hold values from -0.125 to 0.125
- key_weight: bfloat16 [2048, 1024], P('fs', 'tp'), may hold values from -0.125 to 0.125
- value_weight: bfloat16 [2048, 2048], P('fs', 'tp'), may hold values from -0.125 to 0.125
- gate_weight: bfloat16 [2048, 2048], P('fs', 'tp'), may hold values from -0.125 to 0.125
- decay_rate: float32 [8], P('tp'), may hold values from 0.0006510417 to 0.05
- out_weight: bfloat16 [2048, 2048], P('tp', 'fs'), may hold values from -0.125 to 0.125
- gain_mlp: bfloat16 [2048], replicated, may hold values from 0.099609375 to 1.8984375
- up_weight: bfloat16 [2048, 8192], P('fs', 'tp'), may hold values from -0.125 to 0.125
- down_weight: bfloat16 [8192, 2048], P('tp', 'fs'), may hold values from -0.0625 to 0.0625
Outputs:
- layer_out: bfloat16 [24576, 2048], P(('rep', 'fs'), 'tp')
All inputs are finite; a program needn't handle non-finite values.
Results may differ from a plain program's by a relative error of at most 0.019.
Values may be sent and summed in bfloat16 or wider, within the bound.
A program may use at most 128 MiB of HBM per device.

v0:
```python
import jax
import jax.numpy as jnp
from jax import lax
from jax.sharding import Mesh
from jax.sharding import PartitionSpec as P

DK = 128
DV = 256
BLK = 128
TP = ("tp_0", "tp_1")


epsilon = 1e-06
highest = lax.Precision.HIGHEST


def sent_to_all(x, axis):
    devices = lax.axis_size(axis)
    return lax.all_to_all(jnp.broadcast_to(x[None], (devices, *x.shape)), axis, 0, 0, tiled=True)


def laid_out(blocks, dim):
    shape = list(blocks.shape[1:])
    shape[dim] *= blocks.shape[0]
    return jnp.moveaxis(blocks, 0, dim).reshape(shape)


def gather_axes(x, axes, dim):
    far, near = axes
    leading = sent_to_all(x, far)
    blocks = jnp.swapaxes(sent_to_all(leading, near), 0, 1)
    return laid_out(blocks.reshape(-1, *x.shape), dim)


def side_by_side(arrays, axis, dim, along):
    ends, at = ([], 0)
    for a in arrays[:-1]:
        at += a.shape[along]
        ends.append(at)
    both = jnp.concatenate(arrays, axis=along)
    return tuple(jnp.split(lax.all_gather(both, axis, axis=dim, tiled=True), ends, axis=along))


def gather_directly(x, axis, dim):
    return laid_out(sent_to_all(x, axis), dim)


def cut_along(x, dim, devices):
    shape = x.shape
    blocks = x.reshape(*shape[:dim], devices, shape[dim] // devices, *shape[dim + 1 :])
    return jnp.moveaxis(blocks, dim, 0)


def sent_and_summed(x, axis, dim):
    devices = lax.axis_size(axis)
    blocks = lax.all_to_all(cut_along(x, dim, devices), axis, 0, 0, tiled=True)
    return jnp.sum(blocks.astype(jnp.float32), axis=0)


def sum_in_two_steps(x, axes, dim):
    far, near = axes
    blocks = cut_along(x, dim, lax.axis_size(far))
    nearer = sent_and_summed(blocks, near, dim + 1)
    arrived = lax.all_to_all(
        nearer.astype(jnp.bfloat16), far, split_axis=0, concat_axis=0, tiled=True
    )
    return arrived.astype(jnp.float32).sum(axis=0)


def rows_first(arrays, axis, dims):
    turned = [jnp.moveaxis(a, dim, 0) for a, dim in zip(arrays, dims)]
    both = jnp.concatenate([t.reshape(len(t), -1) for t in turned], axis=1)
    filled, at, gathered = (lax.all_gather(both, axis, axis=0, tiled=True), 0, [])
    for t, dim in zip(turned, dims):
        share = filled[:, at : at + t[0].size].reshape(-1, *t.shape[1:])
        gathered.append(jnp.moveaxis(share, 0, dim))
        at += t[0].size
    return tuple(gathered)


def rms_rows(rows, gain):
    values = rows.astype(jnp.float32)
    scaled = values * lax.rsqrt(jnp.mean(values * values, axis=-1, keepdims=True) + epsilon)
    return (scaled * gain.astype(jnp.float32)).astype(jnp.bfloat16)


def retain(query, keys, values, rate, block):
    length, head_count, key_width = query.shape
    value_width = values.shape[-1]
    block_count = length // block
    log_decay = -rate
    positions = jnp.arange(block, dtype=jnp.float32)
    distance = positions[:, None] - positions[None, :]
    causal = distance >= 0
    inside = jnp.where(
        causal[None],
        jnp.exp(log_decay[:, None, None] * jnp.where(causal, distance, 0.0)[None]),
        0.0,
    )
    key_scale = jnp.exp(log_decay[None, :] * (block - 1.0 - positions)[:, None])
    query_scale = jnp.exp(log_decay[None, :] * (positions + 1.0)[:, None])
    carry_decay = jnp.exp(log_decay * block)
    query_blocks = query.reshape(block_count, block, head_count, key_width)
    key_blocks = keys.reshape(block_count, block, head_count, key_width) * key_width ** (-0.5)
    value_blocks = values.reshape(block_count, block, head_count, value_width)

    def advance(state, blocks):
        q_block, k_block, v_block = blocks
        scores = jnp.einsum("ihd,jhd->hij", q_block, k_block, precision=highest) * inside
        inner = jnp.einsum("hij,jhe->ihe", scores, v_block, precision=highest)
        cross = (
            jnp.einsum("ihd,hde->ihe", q_block, state, precision=highest) * query_scale[:, :, None]
        )
        update = jnp.einsum(
            "jhd,jhe->hde", k_block * key_scale[:, :, None], v_block, precision=highest
        )
        return (state * carry_decay[:, None, None] + update, inner + cross)

    initial = jnp.zeros((head_count, key_width, value_width), jnp.float32)
    _, results = lax.scan(advance, initial, (query_blocks, key_blocks, value_blocks))
    return results.reshape(length, head_count, value_width)


def gated_heads(retained, gate):
    length, head_count, value_width = retained.shape
    normed = retained * lax.rsqrt(jnp.mean(retained * retained, axis=-1, keepdims=True) + epsilon)
    gated = jax.nn.silu(gate.reshape(length, head_count, value_width)) * normed
    return gated.reshape(length, head_count * value_width).astype(jnp.bfloat16)


def add_rows(left, piece):
    return jnp.dot(left, piece, preferred_element_type=jnp.float32)


def local(
    tokens,
    gain_mix,
    query_weight,
    key_weight,
    value_weight,
    gate_weight,
    decay_rate,
    out_weight,
    gain_mlp,
    up_weight,
    down_weight,
):
    length = tokens.shape[0]
    whole_rows = gather_axes(tokens, ("tp_0", "tp_1"), 1)
    normed = rms_rows(whole_rows, gain_mix)
    pieces = side_by_side((query_weight, key_weight, value_weight, gate_weight), "fs", 0, 1)
    query, keys, values, gate = tuple((add_rows(normed, pieces[slot]) for slot in range(4)))
    head_local = decay_rate.shape[0]
    retained = retain(
        query.reshape(length, head_local, DK),
        keys.reshape(length, head_local, DK),
        values.reshape(length, head_local, DV),
        decay_rate,
        BLK,
    )
    hidden = gated_heads(retained, gate)
    mix_terms = jnp.dot(
        hidden, gather_directly(out_weight, "fs", 1), preferred_element_type=jnp.float32
    )
    mix_share = sum_in_two_steps(mix_terms.astype(jnp.bfloat16), ("tp_0", "tp_1"), 1)
    mixed = (tokens.astype(jnp.float32) + mix_share).astype(jnp.bfloat16)
    mixed_rows = gather_axes(mixed, ("tp_0", "tp_1"), 1)
    normed_mlp = rms_rows(mixed_rows, gain_mlp)
    up_whole, down_whole = rows_first((up_weight, down_weight), "fs", (0, 1))
    upward = jnp.dot(normed_mlp, up_whole, preferred_element_type=jnp.float32)
    active = jnp.square(jax.nn.relu(upward)).astype(jnp.bfloat16)
    mlp_terms = jnp.dot(active, down_whole, preferred_element_type=jnp.float32)
    mlp_share = sum_in_two_steps(mlp_terms.astype(jnp.bfloat16), ("tp_0", "tp_1"), 1)
    return (mixed.astype(jnp.float32) + mlp_share).astype(jnp.bfloat16)


def solution(mesh):
    finer = Mesh(
        mesh.devices.reshape(mesh.shape["rep"], mesh.shape["fs"], 4, 2),
        ("rep", "fs", "tp_0", "tp_1"),
    )
    placed = (
        P(("rep", "fs"), TP),
        P(),
        P("fs", TP),
        P("fs", TP),
        P("fs", TP),
        P("fs", TP),
        P(TP),
        P(TP, "fs"),
        P(),
        P("fs", TP),
        P(TP, "fs"),
    )
    return jax.shard_map(
        local, mesh=finer, in_specs=placed, out_specs=P(("rep", "fs"), TP), check_vma=False
    )
```

profile of v0, /device:TPU:1, one launch (start us, length us, event | category | flops | bytes accessed | tf_op | source)
XLA Modules:
  0.0 300.0 jit_solution(6761433969810139792)
XLA Ops:
  6.5 1.6 pad_maximum_fusion.1
  8.2 2.3 broadcast_in_dim.21
  10.6 5.0 %all-to-all-start = ((bf16[4,768,256]{2,1,0:T(8,128)(2,1)}), bf16[4,768,256]{2,1,0:T(8,128)(2,1)S(1)}, u32[]{:S(2)}, u32[]{:S(2)}) async-start(bf16[4,768,256]{2,1,0:T(8,128)(2,1)} %broadcast_in_dim.21), calls=%async_computation | async-start | bytes 3145728 | tf_op jit(solution)/shard_map/all_to_all | solution.py:19
  15.7 0.8 pad_maximum_fusion
  17.5 17.3 %all-to-all-done = bf16[4,768,256]{2,1,0:T(8,128)(2,1)S(1)} async-done(((bf16[4,768,256]{2,1,0:T(8,128)(2,1)}), bf16[4,768,256]{2,1,0:T(8,128)(2,1)S(1)}, u32[]{:S(2)}, u32[]{:S(2)}) %all-to-all-start) | async-done | bytes 1572896 | tf_op jit(solution)/shard_map/all_to_all | solution.py:19
  34.7 1.2 copy.75
  36.0 0.8 broadcast_in_dim.22
  36.8 8.4 %all_to_all.45 = bf16[2,4,768,256]{3,1,2,0:T(4,128)(2,1)S(1)} all-to-all(bf16[2,4,768,256]{3,1,2,0:T(4,128)(2,1)S(1)} %broadcast_in_dim.22), channel_id=1, replica_groups=mesh['rep'=2,'fs'=16,'tp_0'=4,'tp_1'=2] {'tp_1'}, dimensions={0} | all-to-all | bytes 6291456 | tf_op jit(solution)/shard_map/all_to_all | solution.py:19
  45.2 1.1 broadcast_in_dim.25
  46.2 8.2 %all-to-all-start.2 = ((bf16[16,256,128]{1,2,0:T(8,128)(2,1)}), bf16[16,256,128]{1,2,0:T(8,128)(2,1)}, u32[]{:S(2)}, u32[]{:S(2)}) async-start(bf16[16,256,128]{1,2,0:T(8,128)(2,1)} %broadcast_in_dim.25), calls=%async_computation.2 | async-start | bytes 2097152 | tf_op jit(solution)/shard_map/all_to_all | solution.py:19
  55.1 2.6 copy-done
  57.7 6.2 %copy.78 = f32[768,8,256]{2,1,0:T(8,128)} copy(f32[768,8,256]{2,0,1:T(8,128)S(1)} %bitcast.166) | data formatting | bytes 12582912 | tf_op jit(solution)/shard_map/convert_element_type | solution.py:82
  63.9 6.6 %copy.77 = f32[768,8,256]{0,2,1:T(8,128)} copy(f32[768,8,256]{2,0,1:T(8,128)} %bitcast.167) | data formatting | bytes 12582912 | tf_op jit(solution)/shard_map/convert_element_type | solution.py:82
  70.6 7.1 %reshape.293 = f32[6,128,2048]{2,1,0:T(8,128)} reshape(f32[768,8,256]{2,1,0:T(8,128)} %copy.78) | data formatting | bytes 12582912 | tf_op jit(solution)/shard_map/convert_element_type | solution.py:82
  78.4 3.7 %multiply_convert_fusion = bf16[6,128,2048]{2,1,0:T(8,128)(2,1)S(1)} fusion(f32[6,128,2048]{2,1,0:T(8,128)} %reshape.293, f32[2048]{0:T(1024)S(1)} %convert_element_type.123, f32[6,128]{1,0:T(8,128)S(1)} %get-tuple-element.211), kind=kLoop, calls=%fused_computation.41 | loop fusion | flops 4718592 | bytes 9448448 | tf_op jit(solution)/shard_map/convert_element_type | solution.py:84
  82.6 2.3 fusion.28
  84.9 9.1 %all-gather.3.cloned.1.call-done = bf16[2048,768]{1,0:T(8,128)(2,1)} async-done(((bf16[128,768]{1,0:T(8,128)(2,1)}), bf16[2048,768]{1,0:T(8,128)(2,1)}) %all-gather.3.cloned.1.call-update) | async-done | bytes 3145744 | tf_op jit(solution)/shard_map/all_gather | solution.py:41
  94.0 2.9 fusion.44
  97.0 1.7 convolution_multiply_fusion.1
  98.7 1.9 convolution_bitcast_fusion.3
  100.5 30.3 %while.15 = (s32[]{:T(128)}, f32[1,128,256]{2,1,0:T(8,128)S(1)}, f32[6,128,1,256]{1,3,2,0:T(8,128)}, f32[1]{0:T(128)}, f32[6,128,1,128]{3,2,1,0:T(1,128)}, /*ind...) while((s32[]{:T(128)}, f32[1,128,256]{2,1,0:T(8,128)S(1)}, ...), condition=%wide.region_2.3_spmd.clone.clone.clone, body=%wide.region_1.2_spmd.clone.clone.clone.sunk | while | flops 176472576 | bytes 1773696 | solution.py:120
  100.6 1.1 broadcast_multiply_fusion.2
  102.3 1.9 fusion.80
  104.3 1.3 fusion.78
  105.6 1.1 broadcast_multiply_fusion.2
  107.4 1.9 fusion.80
  109.3 1.3 fusion.78
  110.6 1.1 broadcast_multiply_fusion.2
  112.4 1.9 fusion.80
  114.3 1.3 fusion.78
  115.6 1.1 broadcast_multiply_fusion.2
  117.4 1.9 fusion.80
  119.3 1.3 fusion.78
  120.6 1.1 broadcast_multiply_fusion.2
  122.4 1.9 fusion.80
  124.3 1.3 fusion.78
  125.6 1.1 broadcast_multiply_fusion.2
  127.4 1.9 fusion.80
  129.4 1.3 fusion.78
  130.8 1.4 copy.82
  132.3 1.2 multiply_reduce_fusion.2
  133.5 3.3 %fusion.41 = bf16[768,256]{1,0:T(8,128)(2,1)S(1)} fusion(f32[6,128,1,256]{3,1,0,2:T(8,128)S(1)} %copy.82, bf16[768,2048]{0,1:T(8,128)(2,1)} %fusion.28, bf16[2048,768]{1,0:T(8,128)(2,1)} %all-gather.3.cloned.1.call-done, f32[768]{0:T(1024)S(1)} %rsqrt_bitcast_fusion), kind=kOutput, calls=%fused_computation.60 | convolution fusion | flops 806682624 | bytes 5377024 | tf_op jit(solution)/shard_map/dot_general | solution.py:132
  136.8 2.2 convolution_convert_fusion
  139.1 2.9 copy.96
  142.0 4.5 %copy.85 = bf16[2,4,768,256]{3,1,2,0:T(4,128)(2,1)S(1)} copy(bf16[2,4,768,256]{2,3,0,1:T(8,128)(2,1)} %bitcast.173) | data formatting | bytes 6291456 | tf_op jit(solution)/shard_map/transpose | solution.py:51
  146.5 17.5 %all_to_all.46 = bf16[2,4,768,256]{3,1,2,0:T(4,128)(2,1)} all-to-all(bf16[2,4,768,256]{3,1,2,0:T(4,128)(2,1)S(1)} %copy.85), channel_id=1, replica_groups=mesh['rep'=2,'fs'=16,'tp_0'=4,'tp_1'=2] {'tp_1'}, dimensions={0} | all-to-all | bytes 6291456 | tf_op jit(solution)/shard_map/all_to_all | solution.py:56
  164.0 4.4 %reduce_sum.71 = bf16[4,768,256]{2,0,1:T(4,128)(2,1)S(1)} reduce(bf16[2,4,768,256]{3,1,2,0:T(4,128)(2,1)} %all_to_all.46, bf16[]{:T(256)} %constant.43.clone.1), dimensions={0}, to_apply=%region_4.5 | reduce | flops 786432 | bytes 4718594 | tf_op jit(solution)/shard_map/reduce_sum | solution.py:57
  168.6 23.0 %all_to_all.47 = bf16[4,768,256]{2,1,0:T(8,128)(2,1)S(1)} all-to-all(bf16[4,768,256]{2,1,0:T(8,128)(2,1)S(1)} %copy.87), channel_id=1, replica_groups=mesh['rep'=2,'fs'=16,'tp_0'=4,'tp_1'=2] {'tp_0'}, dimensions={0} | all-to-all | bytes 3145728 | tf_op jit(solution)/shard_map/all_to_all | solution.py:64
  192.0 1.3 broadcast_in_dim.26
  193.3 3.6 %all-to-all-start.5 = ((bf16[4,768,256]{2,1,0:T(8,128)(2,1)}), bf16[4,768,256]{2,1,0:T(8,128)(2,1)S(1)}, u32[]{:S(2)}, u32[]{:S(2)}) async-start(bf16[4,768,256]{2,1,0:T(8,128)(2,1)} %broadcast_in_dim.26), calls=%async_computation.5 | async-start | bytes 3145728 | tf_op jit(solution)/shard_map/all_to_all | solution.py:19
  196.9 19.4 %all-to-all-done.5 = bf16[4,768,256]{2,1,0:T(8,128)(2,1)S(1)} async-done(((bf16[4,768,256]{2,1,0:T(8,128)(2,1)}), bf16[4,768,256]{2,1,0:T(8,128)(2,1)S(1)}, u32[]{:S(2)}, u32[]{:S(2)}) %all-to-all-start.5) | async-done | bytes 1572896 | tf_op jit(solution)/shard_map/all_to_all | solution.py:19
  216.5 8.2 %all_to_all.48 = bf16[2,4,768,256]{3,2,1,0:T(8,128)(2,1)S(1)} all-to-all(bf16[2,4,768,256]{3,2,1,0:T(8,128)(2,1)S(1)} %broadcast_in_dim.27), channel_id=1, replica_groups=mesh['rep'=2,'fs'=16,'tp_0'=4,'tp_1'=2] {'tp_1'}, dimensions={0} | all-to-all | bytes 6291456 | tf_op jit(solution)/shard_map/all_to_all | solution.py:19
  224.7 3.3 %copy_convert_fusion = f32[2,4,768,256]{3,2,0,1:T(8,128)} fusion(bf16[2,4,768,256]{3,2,1,0:T(8,128)(2,1)S(1)} %all_to_all.48), kind=kLoop, calls=%fused_computation.48 | loop fusion | flops 1572864 | bytes 9437184 | tf_op jit(solution)/shard_map/convert_element_type | solution.py:82
  228.0 6.5 %copy.89 = f32[768,8,256]{0,2,1:T(8,128)} copy(f32[768,8,256]{2,0,1:T(8,128)} %bitcast.170) | data formatting | bytes 12582912 | tf_op jit(solution)/shard_map/convert_element_type | solution.py:82
  235.2 3.4 %fusion.26 = bf16[768,2048]{0,1:T(8,128)(2,1)S(1)} fusion(f32[768,8,256]{0,2,1:T(8,128)} %copy.89, f32[2048]{0:T(1024)S(1)} %convert_element_type.139, f32[768]{0:T(1024)S(1)} %add_rsqrt_fusion), kind=kLoop, calls=%fused_computation.35 | loop fusion | flops 4718592 | bytes 9448448 | tf_op jit(solution)/shard_map/convert_element_type | solution.py:84
  238.6 5.8 %multiply_convert_fusion.1 = bf16[768,1024]{1,0:T(8,128)(2,1)S(1)} fusion(bf16[768,2048]{0,1:T(8,128)(2,1)S(1)} %fusion.26, bf16[2048,2048]{0,1:T(8,128)(2,1)} %all-gather.5.cloned.1.call-done), kind=kOutput, calls=%fused_computation.51 | convolution fusion | flops 3223584768 | bytes 8912896 | tf_op jit(solution)/shard_map/dot_general | solution.py:170
  244.4 4.8 %fusion.33 = bf16[768,2048]{1,0:T(8,128)(2,1)} fusion(bf16[768,1024]{1,0:T(8,128)(2,1)S(1)} %multiply_convert_fusion.1, bf16[2048,2048]{0,1:T(8,128)(2,1)S(1)} %copy-done.7), kind=kOutput, calls=%fused_computation.46 | convolution fusion | flops 3222798336 | bytes 8912896 | tf_op jit(solution)/shard_map/dot_general | solution.py:172
  249.3 3.2 %copy.97 = bf16[768,2048]{0,1:T(8,128)(2,1)S(1)} copy(bf16[768,2048]{1,0:T(8,128)(2,1)} %fusion.33) | data formatting | bytes 6291456 | tf_op jit(solution)/shard_map/reshape | solution.py:50
  252.4 3.6 %copy.92 = bf16[2,4,768,256]{3,1,2,0:T(4,128)(2,1)} copy(bf16[2,4,768,256]{2,3,0,1:T(8,128)(2,1)S(1)} %bitcast.174) | data formatting | bytes 6291456 | tf_op jit(solution)/shard_map/transpose | solution.py:51
  256.1 7.4 %all_to_all.49 = bf16[2,4,768,256]{3,1,2,0:T(4,128)(2,1)S(1)} all-to-all(bf16[2,4,768,256]{3,1,2,0:T(4,128)(2,1)} %copy.92), channel_id=1, replica_groups=mesh['rep'=2,'fs'=16,'tp_0'=4,'tp_1'=2] {'tp_1'}, dimensions={0} | all-to-all | bytes 6291456 | tf_op jit(solution)/shard_map/all_to_all | solution.py:56
  263.5 4.1 %reduce_sum.74 = bf16[4,768,256]{2,0,1:T(4,128)(2,1)} reduce(bf16[2,4,768,256]{3,1,2,0:T(4,128)(2,1)S(1)} %all_to_all.49, bf16[]{:T(256)} %constant.43.clone.1), dimensions={0}, to_apply=%region_7.8 | reduce | flops 786432 | bytes 4718594 | tf_op jit(solution)/shard_map/reduce_sum | solution.py:57
  267.6 1.6 copy.94
  269.2 22.9 %all_to_all.50 = bf16[4,768,256]{2,1,0:T(8,128)(2,1)S(1)} all-to-all(bf16[4,768,256]{2,1,0:T(8,128)(2,1)S(1)} %copy.94), channel_id=1, replica_groups=mesh['rep'=2,'fs'=16,'tp_0'=4,'tp_1'=2] {'tp_0'}, dimensions={0} | all-to-all | bytes 3145728 | tf_op jit(solution)/shard_map/all_to_all | solution.py:64
  292.3 0.9 add_convert_fusion
  (69 shorter events, 7.9 us)
Async XLA Ops:
  6.5 9.0 %copy-start.2 = (bf16[128,1024]{1,0:T(8,128)(2,1)S(1)}, bf16[128,1024]{1,0:T(8,128)(2,1)}, u32[]{:S(2)}) copy-start(bf16[128,1024]{1,0:T(8,128)(2,1)} %param.22) | copy-start | bytes 786436
  6.5 9.2 %copy-start.3 = (bf16[1024,128]{1,0:T(8,128)(2,1)S(1)}, bf16[1024,128]{1,0:T(8,128)(2,1)}, u32[]{:S(2)}) copy-start(bf16[1024,128]{1,0:T(8,128)(2,1)} %param.23) | copy-start | bytes 786436
  6.5 87.5 %all-gather.3.cloned.1.call-start = ((), (), s32[]{:S(2)}) async-start(), calls=%async_computation.9 | async-start | bytes 3342336 | tf_op jit(solution)/shard_map/all_gather | solution.py:41
  8.2 8.4 %copy-start.5 = (bf16[2048]{0:T(1024)(128)(2,1)S(1)}, bf16[2048]{0:T(1024)(128)(2,1)}, u32[]{:S(2)}) copy-start(bf16[2048]{0:T(1024)(128)(2,1)} %param.14) | copy-start | bytes 12292
  8.2 9.1 %copy-start.4 = (bf16[256,128]{1,0:T(8,128)(2,1)S(1)}, bf16[256,128]{1,0:T(8,128)(2,1)}, u32[]{:S(2)}) copy-start(bf16[256,128]{1,0:T(8,128)(2,1)} %param.20) | copy-start | bytes 196612
  10.6 24.2 %all-to-all-start = ((bf16[4,768,256]{2,1,0:T(8,128)(2,1)}), bf16[4,768,256]{2,1,0:T(8,128)(2,1)S(1)}, u32[]{:S(2)}, u32[]{:S(2)}) async-start(bf16[4,768,256]{2,1,0:T(8,128)(2,1)} %broadcast_in_dim.21), calls=%async_computation | async-start | bytes 3145728 | tf_op jit(solution)/shard_map/all_to_all | solution.py:19
  15.6 223.1 %all-gather.5.cloned.1.call-start = ((), (), s32[]{:S(2)}) async-start(), calls=%async_computation.10 | async-start | bytes 8912896 | tf_op jit(solution)/shard_map/all_gather | solution.py:73
  46.2 90.6 %all-to-all-start.2 = ((bf16[16,256,128]{1,2,0:T(8,128)(2,1)}), bf16[16,256,128]{1,2,0:T(8,128)(2,1)}, u32[]{:S(2)}, u32[]{:S(2)}) async-start(bf16[16,256,128]{1,2,0:T(8,128)(2,1)} %broadcast_in_dim.25), calls=%async_computation.2 | async-start | bytes 2097152 | tf_op jit(solution)/shard_map/all_to_all | solution.py:19
  55.1 2.6 copy-start
  77.7 4.5 %slice-start = ((s8[6291456]{0:T(1024)(128)(4,1)}), s8[4194304]{0:T(1024)(128)(4,1)S(1)}, s32[]{:S(2)}) async-start(s8[6291456]{0:T(1024)(128)(4,1)} %bitcast.168), calls=%async_computation.11 | async-start | bytes 8388608
  78.4 4.2 %slice-start.1 = ((s8[6291456]{0:T(1024)(128)(4,1)}), s8[2097152]{0:T(1024)(128)(4,1)S(1)}, s32[]{:S(2)}) async-start(s8[6291456]{0:T(1024)(128)(4,1)} %bitcast.168), calls=%async_computation.12 | async-start | bytes 4194304
  94.0 2.9 copy-start.8
  168.6 23.2 %copy-start.1 = (bf16[768,256]{1,0:T(8,128)(2,1)S(1)}, bf16[768,256]{1,0:T(8,128)(2,1)}, u32[]{:S(2)}) copy-start(bf16[768,256]{1,0:T(8,128)(2,1)} %param.13) | copy-start | bytes 1179652
  191.9 5.0 %copy-start.6 = (bf16[2048]{0:T(1024)(128)(2,1)S(1)}, bf16[2048]{0:T(1024)(128)(2,1)}, u32[]{:S(2)}) copy-start(bf16[2048]{0:T(1024)(128)(2,1)} %param.21) | copy-start | bytes 12292
  193.3 23.0 %all-to-all-start.5 = ((bf16[4,768,256]{2,1,0:T(8,128)(2,1)}), bf16[4,768,256]{2,1,0:T(8,128)(2,1)S(1)}, u32[]{:S(2)}, u32[]{:S(2)}) async-start(bf16[4,768,256]{2,1,0:T(8,128)(2,1)} %broadcast_in_dim.26), calls=%async_computation.5 | async-start | bytes 3145728 | tf_op jit(solution)/shard_map/all_to_all | solution.py:19
  238.6 5.8 %copy-start.7 = (bf16[2048,2048]{0,1:T(8,128)(2,1)S(1)}, bf16[2048,2048]{0,1:T(8,128)(2,1)}, u32[]{:S(2)}) copy-start(bf16[2048,2048]{0,1:T(8,128)(2,1)} %all-gather.5.cloned.1.call-done) | copy-start | bytes 25165828
Sparse Core Ops, SparseCore 0:
  9.1 84.8 all-gather.2
  95.7 123.6 all-gather.4
where the time goes:
time: 302 us; the launch traced here: 300 us
  blocking collectives  87.3 us (29%)
  local copies, waits for them, and re-layouts  54.3 us (18%)
  matrix products  45.9 us (15%)
  waiting for transfers between devices  45.8 us (15%)
  other arithmetic  34.9 us (12%)
  starting transfers between devices  16.8 us (6%)
  between operations  14.4 us (5%)
    all_to_all x2, blocking collectives, sum_in_two_steps(): lax.all_to_all(nearer.astype(jnp.bfloat16), far, split_axis=0, concat_axi...  45.8 us
    all_to_all x3, waiting for transfers between devices, sent_to_all(): lax.all_to_all(jnp.broadcast_to(x[None], (devices, *x.shape)), axis, 0, 0...  36.7 us
    convert_element_type x4, local copies, waits for them, and re-layouts, rms_rows(): values = rows.astype(jnp.float32)  26.5 us
    all_to_all x2, blocking collectives, sent_and_summed(): blocks = lax.all_to_all(cut_along(x, dim, devices), axis, 0, 0, tiled=True)  24.9 us
    all_to_all x3, starting transfers between devices, sent_to_all(): lax.all_to_all(jnp.broadcast_to(x[None], (devices, *x.shape)), axis, 0, 0...  16.8 us
    all_to_all x2, blocking collectives, sent_to_all(): lax.all_to_all(jnp.broadcast_to(x[None], (devices, *x.shape)), axis, 0, 0...  16.6 us
    dot_general x6, matrix products, advance(): inner = jnp.einsum('hij,jhe->ihe', scores, v_block, precision=highest)  11.7 us
    dot_general x4, matrix products, add_rows(): return jnp.dot(left, piece, preferred_element_type=jnp.float32)  9.84 us
  transfers between devices with their start and end apart: 5, of which 3 were waited for; matrix products, arithmetic and copies ran while one was open for 35% of the time, Pallas kernels for 0%

commit v1 on v0

v1 whole, which is shorter than its diff:
```python
import functools

import jax
import jax.numpy as jnp
from jax import lax
from jax.experimental import pallas as pl
from jax.experimental.pallas import tpu as pltpu
from jax.sharding import Mesh
from jax.sharding import PartitionSpec as P

DK = 128
DV = 256
SEQ = 768
D = 2048
CH = 256
NCH = SEQ // CH
HC = CH // 2
EPS = 1e-06
F32 = jnp.float32
BF16 = jnp.bfloat16
TP = ("y", "c")
FS = ("zl", "x")
MESH_ID = pl.DeviceIdType.MESH
N_REMOTE = 160
N_LOCAL = 16


def kernel(
    tok, gmix, qw, kw, vw, gw, rate, ow, gmlp, uw, dw,
    out,
    xg, mg, nrm, wq, wo, wu, wd, kbuf, vbuf, dec, own, snd, prc,
    s_a, s_b, s_p, s_m, r_a, r_b, r_p, r_m, outv,
    send_sem, recv_sem, local_sem,
):
    rep, zl = lax.axis_index("rep"), lax.axis_index("zl")
    x, y, c = lax.axis_index("x"), lax.axis_index("y"), lax.axis_index("c")

    def mod4(v):
        return lax.rem(v + 4, 4)

    def z_id(step):
        z = lax.rem(rep * 4 + zl + step + 8, 8)
        return {"rep": z // 4, "zl": lax.rem(z, 4)}

    xp, xm, x2 = mod4(x + 1), mod4(x - 1), mod4(x + 2)
    zp, zm, z2 = mod4(zl + 1), mod4(zl - 1), mod4(zl + 2)
    yp, ym, y2 = mod4(y + 1), mod4(y - 1), mod4(y + 2)
    to_xp, to_xm = {"x": xp}, {"x": xm}
    to_zp, to_zm = z_id(1), z_id(-1)
    to_yp, to_ym = {"y": yp}, {"y": ym}
    to_pair = {"c": 1 - c}

    ids = {}

    def remote(name, src, dst, dev):
        i = ids.setdefault(name, len(ids))
        return pltpu.make_async_remote_copy(
            src_ref=src,
            dst_ref=dst,
            send_sem=send_sem.at[i],
            recv_sem=recv_sem.at[i],
            device_id=dev,
            device_id_type=MESH_ID,
        )

    sent = []

    def send(name, src, dst, dev):
        copy = remote(name, src, dst, dev)
        copy.start()
        sent.append(copy)

    def arrived(name, dst, dev):
        remote(name, dst, dst, dev).wait_recv()

    local_ids = {}

    def local(name, src, dst):
        i = local_ids.setdefault(name, len(local_ids))
        return pltpu.make_async_copy(src, dst, local_sem.at[i])

    me = y * 2 + c
    wq_own = wq.at[zl, x]
    loads = {
        "tok": local("tok", tok, xg.at[me]),
        "q": local("q", qw, wq_own.at[:, pl.ds(0, DK)]),
        "k": local("k", kw, wq_own.at[:, pl.ds(DK, DK)]),
        "v": local("v", vw, wq_own.at[:, pl.ds(2 * DK, DV)]),
        "g": local("g", gw, wq_own.at[:, pl.ds(2 * DK + DV, DV)]),
        "o": local("o", ow, wo.at[zl, x]),
        "u": local("u", uw, wu.at[zl, x]),
        "d": local("d", dw, wd.at[zl, x]),
    }
    for load in loads.values():
        load.start()

    barrier = pltpu.get_barrier_semaphore()
    for dev in (to_xp, to_xm, to_zp, to_zm, to_yp, to_ym, to_pair):
        pl.semaphore_signal(barrier, inc=1, device_id=dev, device_id_type=MESH_ID)
    pl.semaphore_wait(barrier, 7)

    weights = {"q": (wq, 128), "o": (wo, 256), "u": (wu, 128), "d": (wd, 1024)}

    def rows_of(w, half, quarter=None):
        n = weights[w][1] // 2
        start = 0 if half == "A" else n
        if quarter is None:
            return pl.ds(start, n)
        return pl.ds(start + quarter * (n // 2), n // 2)

    def first_slab(w, half, at, quarter=None):
        buf = weights[w][0]
        rows = rows_of(w, half, quarter)
        return buf.at[zl, at, rows] if half == "A" else buf.at[at, x, rows]

    def second_slab(w, half, at, quarter=None):
        buf = weights[w][0]
        rows = rows_of(w, half, quarter)
        return buf.at[at, :, rows] if half == "A" else buf.at[:, at, rows]

    ring_x = (x, xp, xm, x2, to_xp, to_xm)
    ring_z = (zl, zp, zm, z2, to_zp, to_zm)

    def rings(half):
        return (ring_x, ring_z) if half == "A" else (ring_z, ring_x)

    def w1(w):
        for half in "AB":
            (at, _, _, _, plus, minus), _ = rings(half)
            slab = first_slab(w, half, at)
            send((w, half, "1p"), slab, slab, plus)
            send((w, half, "1m"), slab, slab, minus)

    def w2(w):
        for half in "AB":
            (_, up, dn, _, plus, minus), _ = rings(half)
            arrived((w, half, "1p"), first_slab(w, half, dn), plus)
            slab = first_slab(w, half, dn, 0)
            send((w, half, "2p"), slab, slab, plus)
            arrived((w, half, "1m"), first_slab(w, half, up), minus)
            slab = first_slab(w, half, up, 1)
            send((w, half, "2m"), slab, slab, minus)

    def w3(w):
        for half in "AB":
            (_, _, _, far, plus, minus), (at, _, _, _, plus2, minus2) = rings(half)
            arrived((w, half, "2p"), first_slab(w, half, far, 0), plus)
            arrived((w, half, "2m"), first_slab(w, half, far, 1), minus)
            slab = second_slab(w, half, at)
            send((w, half, "3p"), slab, slab, plus2)
            send((w, half, "3m"), slab, slab, minus2)

    def w4(w):
        for half in "AB":
            _, (_, up, dn, _, plus, minus) = rings(half)
            arrived((w, half, "3p"), second_slab(w, half, dn), plus)
            slab = second_slab(w, half, dn, 0)
            send((w, half, "4p"), slab, slab, plus)
            arrived((w, half, "3m"), second_slab(w, half, up), minus)
            slab = second_slab(w, half, up, 1)
            send((w, half, "4m"), slab, slab, minus)

    def w5(w):
        for half in "AB":
            _, (_, _, _, far, plus, minus) = rings(half)
            arrived((w, half, "4p"), second_slab(w, half, far, 0), plus)
            arrived((w, half, "4m"), second_slab(w, half, far, 1), minus)

    blk = lambda yy, cc: yy * 2 + cc
    other = 1 - c

    def part(buf, b, r, half=None):
        if half is None:
            return buf.at[b, pl.ds(r * CH, CH)]
        return buf.at[b, pl.ds(r * CH + half * HC, HC)]

    def g1(tag, buf, r):
        s = part(buf, blk(y, c), r)
        send((tag, r, "1p"), s, s, to_yp)
        send((tag, r, "1m"), s, s, to_ym)
        send((tag, r, "c0"), s, s, to_pair)

    def g2(tag, buf, r):
        arrived((tag, r, "1p"), part(buf, blk(ym, c), r), to_yp)
        s = part(buf, blk(ym, c), r, 0)
        send((tag, r, "2p"), s, s, to_yp)
        arrived((tag, r, "1m"), part(buf, blk(yp, c), r), to_ym)
        s = part(buf, blk(yp, c), r, 1)
        send((tag, r, "2m"), s, s, to_ym)
        s = part(buf, blk(ym, c), r)
        send((tag, r, "c1"), s, s, to_pair)
        s = part(buf, blk(yp, c), r)
        send((tag, r, "c2"), s, s, to_pair)

    def g3(tag, buf, r):
        s = part(buf, blk(y2, c), r, 0)
        arrived((tag, r, "2p"), s, to_yp)
        send((tag, r, "c3"), s, s, to_pair)
        s = part(buf, blk(y2, c), r, 1)
        arrived((tag, r, "2m"), s, to_ym)
        send((tag, r, "c4"), s, s, to_pair)

    def g4(tag, buf, r):
        arrived((tag, r, "c0"), part(buf, blk(y, other), r), to_pair)
        arrived((tag, r, "c1"), part(buf, blk(ym, other), r), to_pair)
        arrived((tag, r, "c2"), part(buf, blk(yp, other), r), to_pair)
        arrived((tag, r, "c3"), part(buf, blk(y2, other), r, 0), to_pair)
        arrived((tag, r, "c4"), part(buf, blk(y2, other), r, 1), to_pair)

    def rows(r):
        return pl.ds(r * CH, CH)

    def s0(p, r):
        s = snd.at[p, :, rows(r)]
        send(("s", p, r, "0"), s, prc.at[p, :, rows(r)], to_pair)

    def pair_sum(p, r, b, lo, n):
        at = pl.ds(r * CH + lo, n)
        return own[p, b, at, :].astype(F32) + prc[p, b, at, :].astype(F32)

    def s1(p, r):
        arrived(("s", p, r, "0"), prc.at[p, :, rows(r)], to_pair)
        s_a[p, r] = pair_sum(p, r, y2, 0, HC).astype(BF16)
        send(("s", p, r, "1p"), s_a.at[p, r], r_a.at[p, r], to_yp)
        s_b[p, r] = pair_sum(p, r, y2, HC, HC).astype(BF16)
        send(("s", p, r, "1m"), s_b.at[p, r], r_b.at[p, r], to_ym)

    def s2(p, r):
        s_p[p, r, pl.ds(HC, HC)] = pair_sum(p, r, yp, HC, HC).astype(BF16)
        s_m[p, r, pl.ds(0, HC)] = pair_sum(p, r, ym, 0, HC).astype(BF16)
        arrived(("s", p, r, "1p"), r_a.at[p, r], to_yp)
        s_p[p, r, pl.ds(0, HC)] = (
            pair_sum(p, r, yp, 0, HC) + r_a[p, r].astype(F32)
        ).astype(BF16)
        send(("s", p, r, "2p"), s_p.at[p, r], r_p.at[p, r], to_yp)
        arrived(("s", p, r, "1m"), r_b.at[p, r], to_ym)
        s_m[p, r, pl.ds(HC, HC)] = (
            pair_sum(p, r, ym, HC, HC) + r_b[p, r].astype(F32)
        ).astype(BF16)
        send(("s", p, r, "2m"), s_m.at[p, r], r_m.at[p, r], to_ym)

    def s3(p, r):
        total = pair_sum(p, r, y, 0, CH)
        arrived(("s", p, r, "2p"), r_p.at[p, r], to_yp)
        arrived(("s", p, r, "2m"), r_m.at[p, r], to_ym)
        total = total + (r_p[p, r].astype(F32) + r_m[p, r].astype(F32))
        if p == 0:
            mg[me, rows(r), :] = (xg[me, rows(r), :].astype(F32) + total).astype(BF16)
        else:
            outv[rows(r), :] = (mg[me, rows(r), :].astype(F32) + total).astype(BF16)

    def norm(src, gain, r):
        def body(i, carry):
            at = pl.ds(pl.multiple_of(r * CH + i * 64, 64), 64)
            square = jnp.zeros((64, DV), F32)
            for b in range(8):
                v = src[b, at, :].astype(F32)
                square = square + v * v
            mean = jnp.sum(square, axis=-1, keepdims=True) * (1.0 / D)
            scale = lax.rsqrt(mean + EPS)
            for b in range(8):
                v = src[b, at, :].astype(F32)
                g = gain[b : b + 1, :].astype(F32)
                nrm[at, b * DV : (b + 1) * DV] = (v * scale * g).astype(BF16)
            return carry

        lax.fori_loop(0, CH // 64, body, 0, unroll=2)

    def decays():
        rt = rate[0]
        i = lax.broadcasted_iota(jnp.int32, (CH, CH), 0)
        j = lax.broadcasted_iota(jnp.int32, (CH, CH), 1)
        near = (i - j).astype(F32)
        for d in range(NCH):
            dist = near + float(d * CH)
            value = jnp.exp(-rt * jnp.maximum(dist, 0.0)) * DK ** (-0.5)
            dec[d] = jnp.where(dist >= 0.0, value, 0.0)

    def dot(a, b):
        return jnp.dot(a, b, preferred_element_type=F32)

    def scatter_parts(p, r, left, w):
        for b in range(4):
            for dst, cc in ((snd, other), (own, c)):
                right = jnp.concatenate([w[b, 2 * cc], w[b, 2 * cc + 1]], axis=1)
                dst[p, b, rows(r), :] = dot(left, right).astype(BF16)

    def mix(r):
        a = nrm[rows(r), :]
        qkv = dot(a, wq[:, :, :, 0 : 2 * DK + DV].reshape(D, 2 * DK + DV))
        q = qkv[:, :DK].astype(BF16)
        kbuf[rows(r), :] = qkv[:, DK : 2 * DK].astype(BF16)
        vbuf[rows(r), :] = qkv[:, 2 * DK :].astype(BF16)
        gate = dot(a, wq[:, :, :, 2 * DK + DV :].reshape(D, DV))
        kept = jnp.zeros((CH, DV), F32)
        for b in range(r + 1):
            score = lax.dot_general(
                q, kbuf[rows(b), :], (((1,), (1,)), ((), ())), preferred_element_type=F32
            )
            score = (score * dec[r - b]).astype(BF16)
            kept = kept + dot(score, vbuf[rows(b), :])
        mean = jnp.mean(kept * kept, axis=-1, keepdims=True)
        kept = kept * lax.rsqrt(mean + EPS)
        hidden = (gate / (1.0 + jnp.exp(-gate)) * kept).astype(BF16)
        scatter_parts(0, r, hidden, wo)

    def mlp_up(r):
        a = nrm[rows(r), :]
        active = []
        for b in range(4):
            upward = dot(a, wu[:, :, :, b * 256 : (b + 1) * 256].reshape(D, 256))
            upward = jnp.maximum(upward, 0.0)
            active.append((upward * upward).astype(BF16))
        return jnp.concatenate(active, axis=1)

    loads["tok"].wait()
    for r in range(NCH):
        g1("t", xg, r)
    for name in "qkvg":
        loads[name].wait()
    w1("q")
    loads["o"].wait()
    w1("o")
    decays()
    w2("q")
    g2("t", xg, 0)
    loads["u"].wait()
    loads["d"].wait()
    w3("q")
    w2("o")
    g2("t", xg, 1)
    w1("u")
    w3("o")
    g2("t", xg, 2)
    for r in range(NCH):
        g3("t", xg, r)
    w1("d")
    w4("q")
    w2("u")
    w4("o")
    for r in range(NCH):
        g4("t", xg, r)
        norm(xg, gmix, r)
    w3("u")
    w2("d")
    w5("q")
    w5("o")
    mix(0)
    s0(0, 0)
    w3("d")
    mix(1)
    s0(0, 1)
    s1(0, 0)
    mix(2)
    s0(0, 2)
    s2(0, 0)
    s1(0, 1)
    w4("u")
    s1(0, 2)
    s2(0, 1)
    s3(0, 0)
    g1("m", mg, 0)
    s2(0, 2)
    s3(0, 1)
    g1("m", mg, 1)
    g2("m", mg, 0)
    s3(0, 2)
    g1("m", mg, 2)
    g2("m", mg, 1)
    g3("m", mg, 0)
    g2("m", mg, 2)
    g3("m", mg, 1)
    w4("d")
    g4("m", mg, 0)
    norm(mg, gmlp, 0)
    w5("u")
    g3("m", mg, 2)
    active = [mlp_up(0)]
    g4("m", mg, 1)
    norm(mg, gmlp, 1)
    active.append(mlp_up(1))
    g4("m", mg, 2)
    norm(mg, gmlp, 2)
    active.append(mlp_up(2))
    w5("d")
    scatter_parts(1, 0, active[0], wd)
    s0(1, 0)
    scatter_parts(1, 1, active[1], wd)
    s0(1, 1)
    s1(1, 0)
    scatter_parts(1, 2, active[2], wd)
    s0(1, 2)
    s1(1, 1)
    s2(1, 0)
    s1(1, 2)
    s2(1, 1)
    s3(1, 0)
    stores = []
    s2(1, 2)
    s3(1, 1)
    s3(1, 2)
    store = local("out", outv, out)
    store.start()
    for copy in sent:
        copy.wait_send()
    store.wait()


def local(
    tokens, gain_mix, query_weight, key_weight, value_weight, gate_weight,
    decay_rate, out_weight, gain_mlp, up_weight, down_weight,
):
    hbm = pl.BlockSpec(memory_space=pl.ANY)
    vmem = pl.BlockSpec(memory_space=pltpu.VMEM)
    smem = pl.BlockSpec(memory_space=pltpu.SMEM)
    half = lambda n, w: pltpu.VMEM((2, NCH, n, w), BF16)
    return pl.pallas_call(
        kernel,
        out_shape=jax.ShapeDtypeStruct((SEQ, DV), BF16),
        in_specs=[hbm, vmem, hbm, hbm, hbm, hbm, smem, hbm, vmem, hbm, hbm],
        out_specs=hbm,
        scratch_shapes=[
            pltpu.VMEM((8, SEQ, DV), BF16),
            pltpu.VMEM((8, SEQ, DV), BF16),
            pltpu.VMEM((SEQ, D), BF16),
            pltpu.VMEM((4, 4, 128, 768), BF16),
            pltpu.VMEM((4, 4, 256, 128), BF16),
            pltpu.VMEM((4, 4, 128, 1024), BF16),
            pltpu.VMEM((4, 4, 1024, 128), BF16),
            pltpu.VMEM((SEQ, DK), BF16),
            pltpu.VMEM((SEQ, DV), BF16),
            pltpu.VMEM((NCH, CH, CH), F32),
            pltpu.VMEM((2, 4, SEQ, DV), BF16),
            pltpu.VMEM((2, 4, SEQ, DV), BF16),
            pltpu.VMEM((2, 4, SEQ, DV), BF16),
            half(HC, DV), half(HC, DV), half(CH, DV), half(CH, DV),
            half(HC, DV), half(HC, DV), half(CH, DV), half(CH, DV),
            pltpu.VMEM((SEQ, DV), BF16),
            pltpu.SemaphoreType.DMA((N_REMOTE,)),
            pltpu.SemaphoreType.DMA((N_REMOTE,)),
            pltpu.SemaphoreType.DMA((N_LOCAL,)),
        ],
        compiler_params=pltpu.CompilerParams(
            collective_id=0, has_side_effects=True, vmem_limit_bytes=62 * 1024 * 1024
        ),
    )(
        tokens, gain_mix.reshape(8, DV), query_weight, key_weight, value_weight, gate_weight,
        decay_rate, out_weight, gain_mlp.reshape(8, DV), up_weight, down_weight,
    )


def solution(mesh):
    finer = Mesh(
        mesh.devices.reshape(mesh.shape["rep"], 4, 4, 4, 2), ("rep", "zl", "x", "y", "c")
    )
    placed = (
        P(("rep", "zl", "x"), TP), P(), P(FS, TP), P(FS, TP), P(FS, TP), P(FS, TP),
        P(TP), P(TP, FS), P(), P(FS, TP), P(TP, FS),
    )
    return jax.shard_map(
        local, mesh=finer, in_specs=placed, out_specs=P(("rep", "zl", "x"), TP), check_vma=False
    )
```

time: 302 us -> 121 us (0.40)
  Pallas kernels: 0 us -> 116 us
  blocking collectives: 87.3 us -> 0 us
  local copies, waits for them, and re-layouts: 54.3 us -> 3.66 us
  matrix products: 45.9 us -> 0 us
  waiting for transfers between devices: 45.8 us -> 0 us
  other arithmetic: 34.9 us -> 0 us
  starting transfers between devices: 16.8 us -> 0 us
  between operations: 14.4 us -> 0.67 us
    pallas_call x0 -> x1, Pallas kernels: none -> 116 us  [local(): pl.pallas_call(kernel, out_shape=jax.ShapeDtypeStruct((SEQ, DV), BF16), i...]
    all_to_all x6 -> x0, blocking collectives: 87.3 us -> none  [the longest x2 45.8 us: sum_in_two_steps(): lax.all_to_all(nearer.astype(jnp.bfloat16), far, split_axis=0, concat_axi...]
    dot_general x31 -> x0, matrix products: 45.9 us -> none  [the longest x6 11.7 us: advance(): inner = jnp.einsum('hij,jhe->ihe', scores, v_block, precision=highest)]
    all_to_all x3 -> x0, waiting for transfers between devices: 36.7 us -> none  [sent_to_all(): lax.all_to_all(jnp.broadcast_to(x[None], (devices, *x.shape)), axis, 0, 0...]
    convert_element_type x4 -> x0, local copies, waits for them, and re-layouts: 26.5 us -> none  [rms_rows(): values = rows.astype(jnp.float32)]
    all_to_all x3 -> x0, starting transfers between devices: 16.8 us -> none  [sent_to_all(): lax.all_to_all(jnp.broadcast_to(x[None], (devices, *x.shape)), axis, 0, 0...]
    convert_element_type x9 -> x0, other arithmetic: 14.3 us -> none  [the longest x5 9.46 us: rms_rows(): return (scaled * gain.astype(jnp.float32)).astype(jnp.bfloat16)]
    reduce_sum x7 -> x0, other arithmetic: 11.6 us -> none  [the longest x2 8.52 us: sent_and_summed(): return jnp.sum(blocks.astype(jnp.float32), axis=0)]
  transfers between devices with their start and end apart: 5 -> 0, of which waited for: 3 -> 0; matrix products, arithmetic and copies ran while one was open for 35% -> 0% of each run, Pallas kernels for 0% -> 0%
where the time goes in v1:
time: 121 us; the launch traced here: 120 us
  Pallas kernels  116 us (96%)
  local copies, waits for them, and re-layouts  3.66 us (3%)
    pallas_call x1, Pallas kernels, local(): pl.pallas_call(kernel, out_shape=jax.ShapeDtypeStruct((SEQ, DV), BF16), i...  116 us

profile of v1, /device:TPU:1, one launch (start us, length us, event | category | flops | bytes accessed | tf_op | source)
XLA Modules:
  0.0 120.4 jit_solution(6406181794392451808)
XLA Ops:
  0.7 0.0 copy-start
  0.7 1.3 %reshape.6.gmix = bf16[8,256]{1,0:T(8,128)(2,1)} reshape(bf16[2048]{0:T(1024)(128)(2,1)} %param.12) | data formatting | bytes 8192 | tf_op jit(solution)/shard_map/reshape | solution.py:447
  2.0 0.0 copy-done
  2.0 0.6 reshape.7.gmlp
  2.6 116.0 %shard_map.109 = bf16[768,256]{1,0:T(8,128)(2,1)} custom-call(bf16[768,256]{1,0:T(8,128)(2,1)} %tok.1, bf16[8,256]{1,0:T(8,128)(2,1)} %reshape.6.gmix, bf16[128,128]{1,0:T(8,128)(2,1)} %qw.1, bf16[128,128]{1,0:T(8,128)(2,1)} %kw.1, bf16[128,256]{1,0:T(8,128)(2,1)} %vw.1, bf16[128,256]{1,0:T(8,128)(2,1)} %gw.1, f32[1]{0:T(128)S(6)} %copy.13.rate, ...), custom_call_target="tpu_custom_call" | custom-call | tf_op jit(solution)/shard_map/pallas_call | solution.py:417
  118.6 1.8 %copy.14 = bf16[768,256]{1,0:T(8,128)(2,1)} copy(bf16[768,256]{1,0:T(8,128)(2,1)} %shard_map.109) | data formatting | bytes 786432
Async XLA Ops:
  0.7 1.3 %copy-start = (bf16[2048]{0:T(1024)(128)(2,1)S(1)}, bf16[2048]{0:T(1024)(128)(2,1)}, u32[]{:S(2)}) copy-start(bf16[2048]{0:T(1024)(128)(2,1)} %param.19) | copy-start | bytes 12292

commit v2 on v1

v2 whole, which is shorter than its diff:
```python
import functools

import jax
import jax.numpy as jnp
from jax import lax
from jax.experimental import pallas as pl
from jax.experimental.pallas import tpu as pltpu
from jax.sharding import Mesh
from jax.sharding import PartitionSpec as P

DK = 128
DV = 256
SEQ = 768
D = 2048
CH = 256
NCH = SEQ // CH
HC = CH // 2
EPS = 1e-06
F32 = jnp.float32
BF16 = jnp.bfloat16
TP = ("y", "c")
FS = ("zl", "x")
ORDER = [
    ('load', 't'), ('load', 'o'), ('load', 'ud'), ('w1', 'o', 'B'), ('w1', 'o', 'A'), ('load', 'qkvg'),
    ('w1', 'q', 'A'), ('g1', 't', 0), ('w1', 'q', 'B'), ('w3o', 'q', 'A'), ('w3o', 'q', 'B'), ('decays',),
    ('w2', 'o', 'B'), ('w3o', 'o', 'B'), ('w2', 'o', 'A'), ('w1', 'u', 'B'), ('w2', 'q', 'A'),
    ('w2', 'q', 'B'), ('w3n', 'q', 'B'), ('w3n', 'o', 'B'), ('g1', 't', 2), ('w3n', 'q', 'A'),
    ('w3o', 'o', 'A'), ('g1', 't', 1), ('w3f', 'o', 'B'), ('g2', 't', 2), ('g2', 't', 0), ('w3f', 'q', 'B'),
    ('w3f', 'q', 'A'), ('w4o', 'q', 'B'), ('w3f', 'o', 'A'), ('w3n', 'o', 'A'), ('g2', 't', 1),
    ('w4n', 'o', 'B'), ('w4n', 'q', 'B'), ('w4n', 'q', 'A'), ('g3', 't', 2), ('w4o', 'o', 'B'),
    ('w4f', 'o', 'B'), ('w4f', 'q', 'B'), ('w4f', 'q', 'A'), ('w4o', 'q', 'A'), ('w5o', 'q', 'B'),
    ('g3', 't', 1), ('w4o', 'o', 'A'), ('w1', 'u', 'A'), ('w4f', 'o', 'A'), ('w4n', 'o', 'A'),
    ('w1', 'd', 'A'), ('g3', 't', 0), ('w2', 'u', 'B'), ('g4', 't', 0), ('g4', 't', 1), ('w5n', 'o', 'B'),
    ('norm', 't', 0), ('w5f', 'o', 'B'), ('g4', 't', 2), ('w5n', 'q', 'A'), ('w1', 'd', 'B'),
    ('norm', 't', 1), ('w3o', 'd', 'A'), ('w5o', 'o', 'B'), ('w3n', 'u', 'B'), ('norm', 't', 2),
    ('w5n', 'q', 'B'), ('w5f', 'q', 'B'), ('w5f', 'q', 'A'), ('w3o', 'u', 'A'), ('w5o', 'q', 'A'),
    ('mixa', 0), ('w5f', 'o', 'A'), ('w5o', 'o', 'A'), ('w5n', 'o', 'A'), ('mix', 0), ('s0', 0, 0),
    ('mixa', 1), ('mix', 1), ('w2', 'u', 'A'), ('s0', 0, 1), ('s1', 0, 0), ('mixa', 2), ('mix', 2),
    ('s0', 0, 2), ('w2', 'd', 'B'), ('w3f', 'u', 'B'), ('s1', 0, 1), ('w3n', 'd', 'B'), ('s1', 0, 2),
    ('s2', 0, 0), ('w2', 'd', 'A'), ('w3o', 'u', 'B'), ('w3n', 'u', 'A'), ('w4n', 'u', 'B'),
    ('w3f', 'u', 'A'), ('w3n', 'd', 'A'), ('w3f', 'd', 'B'), ('s2', 0, 1), ('s2', 0, 2), ('s3', 0, 0),
    ('g1', 'm', 0), ('w4n', 'u', 'A'), ('w4o', 'u', 'A'), ('s3', 0, 1), ('g1', 'm', 1), ('w4o', 'u', 'B'),
    ('s3', 0, 2), ('w4f', 'u', 'B'), ('w4f', 'u', 'A'), ('g1', 'm', 2), ('w3o', 'd', 'B'), ('w4n', 'd', 'A'),
    ('g2', 'm', 1), ('w3f', 'd', 'A'), ('g2', 'm', 0), ('w5n', 'u', 'B'), ('g2', 'm', 2), ('w4o', 'd', 'A'),
    ('w5n', 'u', 'A'), ('w4f', 'd', 'B'), ('g3', 'm', 1), ('w5o', 'u', 'A'), ('w5f', 'u', 'A'),
    ('w4n', 'd', 'B'), ('w5f', 'u', 'B'), ('g3', 'm', 0), ('w5o', 'u', 'B'), ('g4', 'm', 1), ('norm', 'm', 1),
    ('up', 1), ('g4', 'm', 0), ('norm', 'm', 0), ('w5n', 'd', 'A'), ('g3', 'm', 2), ('w4o', 'd', 'B'),
    ('down', 1, 1), ('s0', 1, 1), ('up', 0), ('down', 1, 0), ('s0', 1, 0), ('s1', 1, 1), ('g4', 'm', 2),
    ('w4f', 'd', 'A'), ('norm', 'm', 2), ('up', 2), ('s1', 1, 0), ('down', 1, 2), ('w5n', 'd', 'B'),
    ('s0', 1, 2), ('w5f', 'd', 'B'), ('w5o', 'd', 'A'), ('s2', 1, 1), ('w5o', 'd', 'B'), ('s1', 1, 2),
    ('w5f', 'd', 'A'), ('down', 2, 1), ('s0', 2, 1), ('s2', 1, 0), ('down', 2, 2), ('s0', 2, 2),
    ('down', 2, 0), ('s0', 2, 0), ('s1', 2, 1), ('s1', 2, 2), ('s1', 2, 0), ('s2', 1, 2), ('s3', 1, 0),
    ('s3', 1, 1), ('s2', 2, 1), ('s2', 2, 2), ('s2', 2, 0), ('s3', 1, 2), ('s3', 2, 2), ('s3', 2, 1),
    ('s3', 2, 0),
]
MESH_ID = pl.DeviceIdType.MESH
N_REMOTE = 260
N_LOCAL = 16


def kernel(
    tok, gmix, qw, kw, vw, gw, rate, ow, gmlp, uw, dw,
    out,
    xg, mg, nrm, wq, wo, wu, wd, kbuf, vbuf, dec, hid, act, outv,
    send_sem, recv_sem, local_sem, *summing,
):
    sums = [summing[11 * p : 11 * p + 11] for p in range(3)]
    rep, zl = lax.axis_index("rep"), lax.axis_index("zl")
    x, y, c = lax.axis_index("x"), lax.axis_index("y"), lax.axis_index("c")

    def mod4(v):
        return lax.rem(v + 4, 4)

    def z_id(step):
        z = lax.rem(rep * 4 + zl + step + 8, 8)
        return {"rep": z // 4, "zl": lax.rem(z, 4)}

    xp, xm, x2 = mod4(x + 1), mod4(x - 1), mod4(x + 2)
    zp, zm, z2 = mod4(zl + 1), mod4(zl - 1), mod4(zl + 2)
    yp, ym, y2 = mod4(y + 1), mod4(y - 1), mod4(y + 2)
    to_xp, to_xm = {"x": xp}, {"x": xm}
    to_zp, to_zm = z_id(1), z_id(-1)
    to_yp, to_ym = {"y": yp}, {"y": ym}
    to_pair = {"c": 1 - c}

    ids = {}

    def remote(name, src, dst, dev):
        i = ids.setdefault(name, len(ids))
        return pltpu.make_async_remote_copy(
            src_ref=src,
            dst_ref=dst,
            send_sem=send_sem.at[i],
            recv_sem=recv_sem.at[i],
            device_id=dev,
            device_id_type=MESH_ID,
        )

    sent = []

    def send(name, src, dst, dev):
        copy = remote(name, src, dst, dev)
        copy.start()
        sent.append(copy)

    def arrived(name, dst, dev):
        remote(name, dst, dst, dev).wait_recv()

    local_ids = {}

    def local(name, src, dst):
        i = local_ids.setdefault(name, len(local_ids))
        return pltpu.make_async_copy(src, dst, local_sem.at[i])

    me = y * 2 + c
    wq_own = wq.at[zl, x]
    loads = {
        "t": local("t", tok, xg.at[me]),
        "q": local("q", qw, wq_own.at[:, pl.ds(0, DK)]),
        "k": local("k", kw, wq_own.at[:, pl.ds(DK, DK)]),
        "v": local("v", vw, wq_own.at[:, pl.ds(2 * DK, DV)]),
        "g": local("g", gw, wq_own.at[:, pl.ds(2 * DK + DV, DV)]),
        "o": local("o", ow, wo.at[zl, x]),
        "u": local("u", uw, wu.at[zl, x]),
        "d": local("d", dw, wd.at[zl, x]),
    }
    for load in loads.values():
        load.start()

    barrier = pltpu.get_barrier_semaphore()
    for dev in (to_xp, to_xm, to_zp, to_zm, to_yp, to_ym, to_pair):
        pl.semaphore_signal(barrier, inc=1, device_id=dev, device_id_type=MESH_ID)
    pl.semaphore_wait(barrier, 7)

    weights = {"q": (wq, 128), "o": (wo, 256), "u": (wu, 128), "d": (wd, 1024)}

    def slab(w, half, first, second, quarter=None):
        buf, n = weights[w]
        start, size = (0 if half == "A" else n // 2), n // 2
        if quarter is not None:
            size //= 2
            start += quarter * size
        zi, xi = (second, first) if half == "A" else (first, second)
        return buf.at[zi, xi, pl.ds(start, size)]

    ring_x = (x, xp, xm, x2, to_xp, to_xm)
    ring_z = (zl, zp, zm, z2, to_zp, to_zm)

    def rings(half):
        return (ring_x, ring_z) if half == "A" else (ring_z, ring_x)

    def w1(w, half):
        (at, _, _, _, plus, minus), (here, *_) = rings(half)
        s = slab(w, half, at, here)
        send((w, half, "1p"), s, s, plus)
        send((w, half, "1m"), s, s, minus)

    def w2(w, half):
        (_, up, dn, _, plus, minus), (here, *_) = rings(half)
        arrived((w, half, "1p"), slab(w, half, dn, here), plus)
        s = slab(w, half, dn, here, 0)
        send((w, half, "2p"), s, s, plus)
        arrived((w, half, "1m"), slab(w, half, up, here), minus)
        s = slab(w, half, up, here, 1)
        send((w, half, "2m"), s, s, minus)

    def slabs_of(kind, ring):
        at, up, dn, far, _, _ = ring
        return {"o": [("o", at)], "n": [("u", up), ("d", dn)], "f": [("f", far)]}[kind]

    def w3(kind, w, half):
        first, (here, _, _, _, plus, minus) = rings(half)
        if kind == "f":
            far = first[3]
            arrived((w, half, "2p"), slab(w, half, far, here, 0), first[4])
            arrived((w, half, "2m"), slab(w, half, far, here, 1), first[5])
        for tag, i in slabs_of(kind, first):
            s = slab(w, half, i, here)
            send((w, half, "3p", tag), s, s, plus)
            send((w, half, "3m", tag), s, s, minus)

    def w4(kind, w, half):
        first, (_, up, dn, _, plus, minus) = rings(half)
        for tag, i in slabs_of(kind, first):
            arrived((w, half, "3p", tag), slab(w, half, i, dn), plus)
            s = slab(w, half, i, dn, 0)
            send((w, half, "4p", tag), s, s, plus)
            arrived((w, half, "3m", tag), slab(w, half, i, up), minus)
            s = slab(w, half, i, up, 1)
            send((w, half, "4m", tag), s, s, minus)

    def w5(kind, w, half):
        first, (_, _, _, far, plus, minus) = rings(half)
        for tag, i in slabs_of(kind, first):
            arrived((w, half, "4p", tag), slab(w, half, i, far, 0), plus)
            arrived((w, half, "4m", tag), slab(w, half, i, far, 1), minus)

    blk = lambda yy, cc: yy * 2 + cc
    other = 1 - c

    def part(buf, b, r, half=None):
        if half is None:
            return buf.at[b, pl.ds(r * CH, CH)]
        return buf.at[b, pl.ds(r * CH + half * HC, HC)]

    def g1(tag, buf, r):
        s = part(buf, blk(y, c), r)
        send((tag, r, "1p"), s, s, to_yp)
        send((tag, r, "1m"), s, s, to_ym)
        send((tag, r, "c0"), s, s, to_pair)

    def g2(tag, buf, r):
        arrived((tag, r, "1p"), part(buf, blk(ym, c), r), to_yp)
        s = part(buf, blk(ym, c), r, 0)
        send((tag, r, "2p"), s, s, to_yp)
        arrived((tag, r, "1m"), part(buf, blk(yp, c), r), to_ym)
        s = part(buf, blk(yp, c), r, 1)
        send((tag, r, "2m"), s, s, to_ym)
        s = part(buf, blk(ym, c), r)
        send((tag, r, "c1"), s, s, to_pair)
        s = part(buf, blk(yp, c), r)
        send((tag, r, "c2"), s, s, to_pair)

    def g3(tag, buf, r):
        s = part(buf, blk(y2, c), r, 0)
        arrived((tag, r, "2p"), s, to_yp)
        send((tag, r, "c3"), s, s, to_pair)
        s = part(buf, blk(y2, c), r, 1)
        arrived((tag, r, "2m"), s, to_ym)
        send((tag, r, "c4"), s, s, to_pair)

    def g4(tag, buf, r):
        arrived((tag, r, "c0"), part(buf, blk(y, other), r), to_pair)
        arrived((tag, r, "c1"), part(buf, blk(ym, other), r), to_pair)
        arrived((tag, r, "c2"), part(buf, blk(yp, other), r), to_pair)
        arrived((tag, r, "c3"), part(buf, blk(y2, other), r, 0), to_pair)
        arrived((tag, r, "c4"), part(buf, blk(y2, other), r, 1), to_pair)

    def rows(r):
        return pl.ds(r * CH, CH)

    def s0(p, r):
        own, snd, prc = sums[p][:3]
        send(("s", p, r, "0"), snd.at[:, rows(r)], prc.at[:, rows(r)], to_pair)

    def pair_sum(p, r, b, lo, n):
        own, snd, prc = sums[p][:3]
        at = pl.ds(r * CH + lo, n)
        return own[b, at, :].astype(F32) + prc[b, at, :].astype(F32)

    def s1(p, r):
        _, _, prc, s_a, s_b, _, _, r_a, r_b, _, _ = sums[p]
        arrived(("s", p, r, "0"), prc.at[:, rows(r)], to_pair)
        s_a[r] = pair_sum(p, r, y2, 0, HC).astype(BF16)
        send(("s", p, r, "1p"), s_a.at[r], r_a.at[r], to_yp)
        s_b[r] = pair_sum(p, r, y2, HC, HC).astype(BF16)
        send(("s", p, r, "1m"), s_b.at[r], r_b.at[r], to_ym)

    def s2(p, r):
        _, _, _, _, _, s_p, s_m, r_a, r_b, r_p, r_m = sums[p]
        s_p[r, pl.ds(HC, HC)] = pair_sum(p, r, yp, HC, HC).astype(BF16)
        s_m[r, pl.ds(0, HC)] = pair_sum(p, r, ym, 0, HC).astype(BF16)
        arrived(("s", p, r, "1p"), r_a.at[r], to_yp)
        s_p[r, pl.ds(0, HC)] = (pair_sum(p, r, yp, 0, HC) + r_a[r].astype(F32)).astype(BF16)
        send(("s", p, r, "2p"), s_p.at[r], r_p.at[r], to_yp)
        arrived(("s", p, r, "1m"), r_b.at[r], to_ym)
        s_m[r, pl.ds(HC, HC)] = (pair_sum(p, r, ym, HC, HC) + r_b[r].astype(F32)).astype(BF16)
        send(("s", p, r, "2m"), s_m.at[r], r_m.at[r], to_ym)

    odd = lax.rem(x, 2)
    column = {1: 1 - odd, 2: odd}
    stores = []

    def s3(p, r):
        r_p, r_m = sums[p][9:]
        total = pair_sum(p, r, y, 0, CH)
        arrived(("s", p, r, "2p"), r_p.at[r], to_yp)
        arrived(("s", p, r, "2m"), r_m.at[r], to_ym)
        total = total + (r_p[r].astype(F32) + r_m[r].astype(F32))
        if p == 0:
            mg[me, rows(r), :] = (xg[me, rows(r), :].astype(F32) + total).astype(BF16)
            return
        mixed = mg[me, rows(r), :]
        mixed = jnp.where(column[p] == 0, mixed[:, :128], mixed[:, 128:]).astype(F32)
        outv[p - 1, rows(r), :] = (mixed + total).astype(BF16)
        columns = pl.ds(pl.multiple_of(column[p] * 128, 128), 128)
        store = local(("out", p, r), outv.at[p - 1, rows(r)], out.at[rows(r), columns])
        store.start()
        stores.append(store)

    def norm(src, gain, r):
        def body(i, carry):
            at = pl.ds(pl.multiple_of(r * CH + i * 64, 64), 64)
            square = jnp.zeros((64, DV), F32)
            for b in range(8):
                v = src[b, at, :].astype(F32)
                square = square + v * v
            mean = jnp.sum(square, axis=-1, keepdims=True) * (1.0 / D)
            scale = lax.rsqrt(mean + EPS)
            for b in range(8):
                v = src[b, at, :].astype(F32)
                g = gain[pl.ds(b * DV, DV)].reshape(1, DV).astype(F32)
                nrm[at, b * DV : (b + 1) * DV] = (v * scale * g).astype(BF16)
            return carry

        lax.fori_loop(0, CH // 64, body, 0, unroll=2)

    def decays():
        rt = rate[0]
        i = lax.broadcasted_iota(jnp.int32, (CH, CH), 0)
        j = lax.broadcasted_iota(jnp.int32, (CH, CH), 1)
        near = (i - j).astype(F32)
        for d in range(NCH):
            dist = near + float(d * CH)
            value = jnp.exp(-rt * jnp.maximum(dist, 0.0)) * DK ** (-0.5)
            dec[d] = jnp.where(dist >= 0.0, value, 0.0)

    def dot(a, b):
        return jnp.dot(a, b, preferred_element_type=F32)

    def mixa(r):
        a = nrm[rows(r), :]
        qkv = dot(a, wq[:, :, :, 0 : 2 * DK + DV].reshape(D, 2 * DK + DV))
        q = qkv[:, :DK].astype(BF16)
        kbuf[rows(r), :] = qkv[:, DK : 2 * DK].astype(BF16)
        vbuf[rows(r), :] = qkv[:, 2 * DK :].astype(BF16)
        gate = dot(a, wq[:, :, :, 2 * DK + DV :].reshape(D, DV))
        kept = jnp.zeros((CH, DV), F32)
        for b in range(r + 1):
            score = lax.dot_general(
                q, kbuf[rows(b), :], (((1,), (1,)), ((), ())), preferred_element_type=F32
            )
            score = (score * dec[r - b]).astype(BF16)
            kept = kept + dot(score, vbuf[rows(b), :])
        mean = jnp.mean(kept * kept, axis=-1, keepdims=True)
        kept = kept * lax.rsqrt(mean + EPS)
        hid[rows(r), :] = (gate / (1.0 + jnp.exp(-gate)) * kept).astype(BF16)

    def mix(r):
        own, snd = sums[0][:2]
        for b in range(4):
            for dst, cc in ((snd, other), (own, c)):
                right = jnp.concatenate([wo[b, 2 * cc], wo[b, 2 * cc + 1]], axis=1)
                dst[b, rows(r), :] = dot(hid[rows(r), :], right).astype(BF16)

    def up(r):
        a = nrm[rows(r), :]
        for b in range(4):
            upward = dot(a, wu[:, :, :, b * 256 : (b + 1) * 256].reshape(D, 256))
            upward = jnp.maximum(upward, 0.0)
            act[rows(r), b * 256 : (b + 1) * 256] = (upward * upward).astype(BF16)

    def down(p, r):
        own, snd = sums[p][:2]
        for b in (0, 2):
            for dst, cc in ((snd, other), (own, c)):
                at = 2 * cc + column[p]
                right = jnp.concatenate([wd[b, at], wd[b + 1, at]], axis=1)
                value = dot(act[rows(r), :], right).astype(BF16)
                dst[b, rows(r), :] = value[:, :128]
                dst[b + 1, rows(r), :] = value[:, 128:]

    def load(names):
        for name in names:
            loads[name].wait()

    feats = {"t": (xg, gmix), "m": (mg, gmlp)}
    kinds = {"w3": w3, "w4": w4, "w5": w5}
    plain = {
        "load": load, "w1": w1, "w2": w2, "s0": s0, "s1": s1, "s2": s2, "s3": s3,
        "mixa": mixa, "mix": mix, "up": up, "down": down, "decays": decays,
    }
    gathers = {"g1": g1, "g2": g2, "g3": g3, "g4": g4}
    for name, *args in ORDER:
        if name == "norm":
            norm(*feats[args[0]], args[1])
        elif name in gathers:
            gathers[name](args[0], feats[args[0]][0], args[1])
        elif name in plain:
            plain[name](*args)
        else:
            kinds[name[:2]](name[2], *args)
    for copy in sent:
        copy.wait_send()
    for store in stores:
        store.wait()


def local(
    tokens, gain_mix, query_weight, key_weight, value_weight, gate_weight,
    decay_rate, out_weight, gain_mlp, up_weight, down_weight,
):
    hbm = pl.BlockSpec(memory_space=pl.ANY)
    vmem = pl.BlockSpec(memory_space=pltpu.VMEM)
    smem = pl.BlockSpec(memory_space=pltpu.SMEM)

    def summing(width):
        whole = [pltpu.VMEM((4, SEQ, width), BF16)] * 3
        moved = [pltpu.VMEM((NCH, n, width), BF16) for n in (HC, HC, CH, CH)]
        return whole + moved + moved

    return pl.pallas_call(
        kernel,
        out_shape=jax.ShapeDtypeStruct((SEQ, DV), BF16),
        in_specs=[hbm, vmem, hbm, hbm, hbm, hbm, smem, hbm, vmem, hbm, hbm],
        out_specs=hbm,
        scratch_shapes=[
            pltpu.VMEM((8, SEQ, DV), BF16),
            pltpu.VMEM((8, SEQ, DV), BF16),
            pltpu.VMEM((SEQ, D), BF16),
            pltpu.VMEM((4, 4, 128, 768), BF16),
            pltpu.VMEM((4, 4, 256, 128), BF16),
            pltpu.VMEM((4, 4, 128, 1024), BF16),
            pltpu.VMEM((4, 4, 1024, 128), BF16),
            pltpu.VMEM((SEQ, DK), BF16),
            pltpu.VMEM((SEQ, DV), BF16),
            pltpu.VMEM((NCH, CH, CH), F32),
            pltpu.VMEM((SEQ, DV), BF16),
            pltpu.VMEM((SEQ, 1024), BF16),
            pltpu.VMEM((2, SEQ, 128), BF16),
            pltpu.SemaphoreType.DMA((N_REMOTE,)),
            pltpu.SemaphoreType.DMA((N_REMOTE,)),
            pltpu.SemaphoreType.DMA((N_LOCAL,)),
            *summing(DV), *summing(128), *summing(128),
        ],
        compiler_params=pltpu.CompilerParams(
            collective_id=0, has_side_effects=True, vmem_limit_bytes=62 * 1024 * 1024
        ),
    )(
        tokens, gain_mix, query_weight, key_weight, value_weight, gate_weight,
        decay_rate, out_weight, gain_mlp, up_weight, down_weight,
    )


def solution(mesh):
    finer = Mesh(
        mesh.devices.reshape(mesh.shape["rep"], 4, 4, 4, 2), ("rep", "zl", "x", "y", "c")
    )
    placed = (
        P(("rep", "zl", "x"), TP), P(), P(FS, TP), P(FS, TP), P(FS, TP), P(FS, TP),
        P(TP), P(TP, FS), P(), P(FS, TP), P(TP, FS),
    )
    return jax.shard_map(
        local, mesh=finer, in_specs=placed, out_specs=P(("rep", "zl", "x"), TP), check_vma=False
    )
```

time: 121 us -> 98.3 us (0.81)
  Pallas kernels: 116 us -> 95.7 us
  local copies, waits for them, and re-layouts: 3.66 us -> 1.77 us
    pallas_call x1, Pallas kernels: 116 us -> 95.7 us  [local(): pl.pallas_call(kernel, out_shape=jax.ShapeDtypeStruct((SEQ, DV), BF16), i...]
    reshape x2 -> x0, local copies, waits for them, and re-layouts: 1.89 us -> none  [the longest x1 1.29 us: local(): gain_mix.reshape(8, DV)]
where the time goes in v2:
time: 98.3 us; the launch traced here: 98.1 us
  Pallas kernels  95.7 us (97%)
  local copies, waits for them, and re-layouts  1.77 us (2%)
    pallas_call x1, Pallas kernels, local(): pl.pallas_call(kernel, out_shape=jax.ShapeDtypeStruct((SEQ, DV), BF16), i...  95.7 us

profile of v2, /device:TPU:1, one launch (start us, length us, event | category | flops | bytes accessed | tf_op | source)
XLA Modules:
  0.0 98.1 jit_solution(5914061815834275455)
XLA Ops:
  0.7 95.7 %shard_map.109 = bf16[768,256]{1,0:T(8,128)(2,1)} custom-call(bf16[768,256]{1,0:T(8,128)(2,1)} %tok.1, bf16[2048]{0:T(1024)(128)(2,1)} %gmix.1, bf16[128,128]{1,0:T(8,128)(2,1)} %qw.1, bf16[128,128]{1,0:T(8,128)(2,1)} %kw.1, bf16[128,256]{1,0:T(8,128)(2,1)} %vw.1, bf16[128,256]{1,0:T(8,128)(2,1)} %gw.1, f32[1]{0:T(128)S(6)} %copy.13.rate, ...), custom_call_target="tpu_custom_call" | custom-call | tf_op jit(solution)/shard_map/pallas_call | solution.py:402
  96.3 1.8 %copy.14 = bf16[768,256]{1,0:T(8,128)(2,1)} copy(bf16[768,256]{1,0:T(8,128)(2,1)} %shard_map.109) | data formatting | bytes 786432

commit v3 on v2

v3 whole, which is shorter than its diff:
```python
import functools

import jax
import jax.numpy as jnp
from jax import lax
from jax.experimental import pallas as pl
from jax.experimental.pallas import tpu as pltpu
from jax.sharding import Mesh
from jax.sharding import PartitionSpec as P

DK = 128
DV = 256
SEQ = 768
D = 2048
CH = 256
NCH = SEQ // CH
HC = CH // 2
EPS = 1e-06
F32 = jnp.float32
BF16 = jnp.bfloat16
TP = ("y", "c")
FS = ("zl", "x")
ORDER = [
    ('load', 'ud'), ('load', 'qkvg'), ('load', 't'), ('w1', 'q', 'B'), ('w1', 'q', 'A'), ('g1', 't', 1),
    ('load', 'o'), ('w1', 'o', 'B'), ('w3o', 'o', 'A'), ('g1', 't', 2), ('w1', 'o', 'A'), ('w3o', 'q', 'B'),
    ('w3o', 'q', 'A'), ('w1', 'u', 'A'), ('g1', 't', 0), ('w3o', 'o', 'B'), ('w1', 'u', 'B'),
    ('w2', 'q', 'A'), ('w2', 'o', 'B'), ('w2', 'o', 'A'), ('w2', 'q', 'B'), ('w3n', 'q', 'A'),
    ('w3n', 'o', 'A'), ('w3n', 'q', 'B'), ('g2', 't', 1), ('w3f', 'o', 'A'), ('w3f', 'q', 'A'),
    ('g3', 't', 1), ('w4o', 'q', 'A'), ('w4o', 'o', 'B'), ('w4o', 'o', 'A'), ('w3f', 'q', 'B'),
    ('w3f', 'o', 'B'), ('w3n', 'o', 'B'), ('decays',), ('g2', 't', 0), ('g4', 't', 1), ('w4n', 'q', 'A'),
    ('w4o', 'q', 'B'), ('g2', 't', 2), ('w4n', 'q', 'B'), ('norm', 't', 1), ('w4f', 'q', 'B'),
    ('w4f', 'q', 'A'), ('w4n', 'o', 'B'), ('w5o', 'o', 'A'), ('w4n', 'o', 'A'), ('g3', 't', 0),
    ('w4f', 'o', 'A'), ('g3', 't', 2), ('w4f', 'o', 'B'), ('g4', 't', 2), ('w3o', 'u', 'B'), ('w2', 'u', 'B'),
    ('g4', 't', 0), ('w5o', 'q', 'A'), ('w1', 'd', 'B'), ('w5n', 'q', 'B'), ('norm', 't', 2),
    ('norm', 't', 0), ('w5f', 'q', 'B'), ('w2', 'u', 'A'), ('w5f', 'q', 'A'), ('w5n', 'q', 'A'),
    ('w5o', 'o', 'B'), ('w3o', 'u', 'A'), ('w5o', 'q', 'B'), ('w1', 'd', 'A'), ('mixa', 0), ('w5n', 'o', 'A'),
    ('w5n', 'o', 'B'), ('w5f', 'o', 'A'), ('w5f', 'o', 'B'), ('mix', 0), ('s0', 0, 0), ('mixa', 1),
    ('w3n', 'u', 'A'), ('mix', 1), ('s0', 0, 1), ('s1', 0, 0), ('w3f', 'u', 'B'), ('mixa', 2), ('mix', 2),
    ('s0', 0, 2), ('s1', 0, 1), ('w3n', 'u', 'B'), ('s1', 0, 2), ('w2', 'd', 'A'), ('s2', 0, 0),
    ('w2', 'd', 'B'), ('s2', 0, 1), ('w4o', 'u', 'B'), ('w3f', 'u', 'A'), ('s2', 0, 2), ('s3', 0, 0),
    ('g1', 'm', 0), ('w4n', 'u', 'A'), ('w3n', 'd', 'A'), ('w3n', 'd', 'B'), ('w4f', 'u', 'B'),
    ('w4f', 'u', 'A'), ('w5o', 'u', 'B'), ('w4o', 'u', 'A'), ('s3', 0, 2), ('g1', 'm', 2), ('w4n', 'u', 'B'),
    ('w3o', 'd', 'A'), ('s3', 0, 1), ('g2', 'm', 0), ('g1', 'm', 1), ('w3f', 'd', 'B'), ('w3o', 'd', 'B'),
    ('g2', 'm', 2), ('w4n', 'd', 'A'), ('w5n', 'u', 'A'), ('w5f', 'u', 'A'), ('w3f', 'd', 'A'),
    ('g3', 'm', 0), ('g2', 'm', 1), ('w5n', 'u', 'B'), ('g4', 'm', 0), ('norm', 'm', 0), ('w4n', 'd', 'B'),
    ('w5f', 'u', 'B'), ('w5o', 'u', 'A'), ('g3', 'm', 2), ('up', 0), ('w4f', 'd', 'B'), ('w4o', 'd', 'A'),
    ('g4', 'm', 2), ('norm', 'm', 2), ('up', 2), ('g3', 'm', 1), ('w5n', 'd', 'A'), ('w4o', 'd', 'B'),
    ('down', 1, 2), ('s0', 1, 2), ('down', 1, 0), ('s0', 1, 0), ('g4', 'm', 1), ('s1', 1, 2),
    ('norm', 'm', 1), ('w4f', 'd', 'A'), ('s1', 1, 0), ('up', 1), ('down', 1, 1), ('w5f', 'd', 'B'),
    ('s0', 1, 1), ('s2', 1, 2), ('s1', 1, 1), ('w5o', 'd', 'A'), ('w5n', 'd', 'B'), ('w5o', 'd', 'B'),
    ('s2', 1, 0), ('w5f', 'd', 'A'), ('down', 2, 2), ('s0', 2, 2), ('down', 2, 1), ('s0', 2, 1), ('s1', 2, 2),
    ('down', 2, 0), ('s1', 2, 1), ('s3', 1, 2), ('s0', 2, 0), ('s2', 1, 1), ('s1', 2, 0), ('s2', 2, 2),
    ('s3', 1, 0), ('s2', 2, 1), ('s3', 1, 1), ('s2', 2, 0), ('s3', 2, 1), ('s3', 2, 2), ('s3', 2, 0),
]
MESH_ID = pl.DeviceIdType.MESH
N_SENDS = 20
N_ARRIVALS = 97
N_LOCAL = 6


def kernel(
    tok, gmix, qw, kw, vw, gw, rate, ow, gmlp, uw, dw,
    out,
    xg, mg, nrm, wq, wo, wu, wd, kbuf, vbuf, dec, hid, act, outv,
    send_sem, recv_sem, local_sem, *summing,
):
    sums = [summing[11 * p : 11 * p + 11] for p in range(3)]
    rep, zl = lax.axis_index("rep"), lax.axis_index("zl")
    x, y, c = lax.axis_index("x"), lax.axis_index("y"), lax.axis_index("c")

    def mod4(v):
        return lax.rem(v + 4, 4)

    def z_id(step):
        z = lax.rem(rep * 4 + zl + step + 8, 8)
        return {"rep": z // 4, "zl": lax.rem(z, 4)}

    xp, xm, x2 = mod4(x + 1), mod4(x - 1), mod4(x + 2)
    zp, zm, z2 = mod4(zl + 1), mod4(zl - 1), mod4(zl + 2)
    yp, ym, y2 = mod4(y + 1), mod4(y - 1), mod4(y + 2)
    to_xp, to_xm = {"x": xp}, {"x": xm}
    to_zp, to_zm = z_id(1), z_id(-1)
    to_yp, to_ym = {"y": yp}, {"y": ym}
    to_pair = {"c": 1 - c}

    sends, arrivals = {}, {}

    def remote(out_group, in_group, src, dst, dev):
        i = sends.setdefault(out_group, len(sends))
        j = arrivals.setdefault(in_group, len(arrivals))
        return pltpu.make_async_remote_copy(
            src_ref=src,
            dst_ref=dst,
            send_sem=send_sem.at[i],
            recv_sem=recv_sem.at[j],
            device_id=dev,
            device_id_type=MESH_ID,
        )

    def send(out_group, in_group, src, dst, dev):
        remote(out_group, in_group, src, dst, dev).start()

    def arrived(in_group, whole, dev):
        remote(next(iter(sends)), in_group, whole, whole, dev).wait_recv()

    me = y * 2 + c
    wq_own = wq.at[zl, x]
    loads = [
        (0, tok, xg.at[me]),
        (1, qw, wq_own.at[:, pl.ds(0, DK)]),
        (1, kw, wq_own.at[:, pl.ds(DK, DK)]),
        (1, vw, wq_own.at[:, pl.ds(2 * DK, DV)]),
        (1, gw, wq_own.at[:, pl.ds(2 * DK + DV, DV)]),
        (2, ow, wo.at[zl, x]),
        (3, uw, wu.at[zl, x]),
        (4, dw, wd.at[zl, x]),
    ]
    for i, src, dst in loads:
        pltpu.make_async_copy(src, dst, local_sem.at[i]).start()

    barrier = pltpu.get_barrier_semaphore()
    for dev in (to_xp, to_xm, to_zp, to_zm, to_yp, to_ym, to_pair):
        pl.semaphore_signal(barrier, inc=1, device_id=dev, device_id_type=MESH_ID)
    pl.semaphore_wait(barrier, 7)

    weights = {"q": (wq, 128), "o": (wo, 256), "u": (wu, 128), "d": (wd, 1024)}

    def slab(w, half, first, second, quarter=None):
        buf, n = weights[w]
        start, size = (0 if half == "A" else n // 2), n // 2
        if quarter is not None:
            size //= 2
            start += quarter * size
        zi, xi = (second, first) if half == "A" else (first, second)
        return buf.at[zi, xi, pl.ds(start, size)]

    ring_x = (x, xp, xm, x2, to_xp, to_xm)
    ring_z = (zl, zp, zm, z2, to_zp, to_zm)

    def rings(half):
        return (ring_x, ring_z) if half == "A" else (ring_z, ring_x)

    def shards(w, n):
        buf = weights[w][0]
        return buf.at[0, pl.ds(0, n)]

    def half_shard(w):
        buf, n = weights[w]
        return buf.at[0, 0, pl.ds(0, n // 2)]

    def w1(w, half):
        (at, _, _, _, plus, minus), (here, *_) = rings(half)
        s = slab(w, half, at, here)
        send((w, "first"), (w, half, 1), s, s, plus)
        send((w, "first"), (w, half, 1), s, s, minus)

    def w2(w, half):
        (_, up, dn, _, plus, minus), (here, *_) = rings(half)
        arrived((w, half, 1), shards(w, 1), plus)
        s = slab(w, half, dn, here, 0)
        send((w, "first"), (w, half, 2), s, s, plus)
        s = slab(w, half, up, here, 1)
        send((w, "first"), (w, half, 2), s, s, minus)

    def slabs_of(kind, ring):
        at, up, dn, far, _, _ = ring
        return {"o": [at], "n": [up, dn], "f": [far]}[kind]

    def w3(kind, w, half):
        first, (here, _, _, _, plus, minus) = rings(half)
        if kind == "f":
            arrived((w, half, 2), half_shard(w), first[4])
        for i in slabs_of(kind, first):
            s = slab(w, half, i, here)
            send((w, "third"), (w, half, 3, kind), s, s, plus)
            send((w, "third"), (w, half, 3, kind), s, s, minus)

    def last_group(kind, w, half):
        return (w, half, 4, kind if w == "d" else "all")

    def w4(kind, w, half):
        first, (_, up, dn, _, plus, minus) = rings(half)
        slabs = slabs_of(kind, first)
        arrived((w, half, 3, kind), shards(w, len(slabs)), plus)
        for i in slabs:
            s = slab(w, half, i, dn, 0)
            send((w, "fourth"), last_group(kind, w, half), s, s, plus)
            s = slab(w, half, i, up, 1)
            send((w, "fourth"), last_group(kind, w, half), s, s, minus)

    seen = {}

    def w5(kind, w, half):
        plus = rings(half)[1][4]
        seen[w, half] = seen.get((w, half), 0) + 1
        if w == "d":
            ref = shards(w, 1) if kind == "n" else half_shard(w)
            arrived(last_group(kind, w, half), ref, plus)
        elif seen[w, half] == 3:
            arrived(last_group(kind, w, half), shards(w, 2), plus)

    def rows(r):
        return pl.ds(r * CH, CH)

    blk = lambda yy, cc: yy * 2 + cc
    other = 1 - c

    def part(buf, b, r, half=None):
        if half is None:
            return buf.at[b, pl.ds(r * CH, CH)]
        return buf.at[b, pl.ds(r * CH + half * HC, HC)]

    def g1(tag, buf, r):
        s = part(buf, blk(y, c), r)
        send(tag, (tag, r, 1), s, s, to_yp)
        send(tag, (tag, r, 1), s, s, to_ym)
        send(tag, (tag, r, 3), s, s, to_pair)

    def g2(tag, buf, r):
        arrived((tag, r, 1), buf.at[pl.ds(0, 2), rows(r)], to_yp)
        s = part(buf, blk(ym, c), r, 0)
        send(tag, (tag, r, 2), s, s, to_yp)
        s = part(buf, blk(yp, c), r, 1)
        send(tag, (tag, r, 2), s, s, to_ym)
        s = part(buf, blk(ym, c), r)
        send(tag, (tag, r, 3), s, s, to_pair)
        s = part(buf, blk(yp, c), r)
        send(tag, (tag, r, 3), s, s, to_pair)

    def g3(tag, buf, r):
        s = part(buf, blk(y2, c), r)
        arrived((tag, r, 2), s, to_yp)
        send(tag, (tag, r, 3), s, s, to_pair)

    def g4(tag, buf, r):
        arrived((tag, r, 3), buf.at[pl.ds(0, 4), rows(r)], to_pair)

    def s0(p, r):
        own, snd, prc = sums[p][:3]
        send(("pair", p), (p, r, 0), snd.at[:, rows(r)], prc.at[:, rows(r)], to_pair)

    def pair_sum(p, r, b, lo, n):
        own, snd, prc = sums[p][:3]
        at = pl.ds(r * CH + lo, n)
        return own[b, at, :].astype(F32) + prc[b, at, :].astype(F32)

    def s1(p, r):
        _, _, prc, s_a, s_b, _, _, r_a, r_b, _, _ = sums[p]
        arrived((p, r, 0), prc.at[:, rows(r)], to_pair)
        s_a[r] = pair_sum(p, r, y2, 0, HC).astype(BF16)
        send(("ring", p), (p, r, 1), s_a.at[r], r_a.at[r], to_yp)
        s_b[r] = pair_sum(p, r, y2, HC, HC).astype(BF16)
        send(("ring", p), (p, r, 1), s_b.at[r], r_b.at[r], to_ym)

    def s2(p, r):
        own, _, _, _, _, s_p, s_m, r_a, r_b, r_p, r_m = sums[p]
        s_p[r, pl.ds(HC, HC)] = pair_sum(p, r, yp, HC, HC).astype(BF16)
        s_m[r, pl.ds(0, HC)] = pair_sum(p, r, ym, 0, HC).astype(BF16)
        arrived((p, r, 1), own.at[0, rows(r)], to_yp)
        s_p[r, pl.ds(0, HC)] = (pair_sum(p, r, yp, 0, HC) + r_a[r].astype(F32)).astype(BF16)
        send(("ring", p), (p, r, 2), s_p.at[r], r_p.at[r], to_yp)
        s_m[r, pl.ds(HC, HC)] = (pair_sum(p, r, ym, HC, HC) + r_b[r].astype(F32)).astype(BF16)
        send(("ring", p), (p, r, 2), s_m.at[r], r_m.at[r], to_ym)

    odd = lax.rem(x, 2)
    column = {1: 1 - odd, 2: odd}

    def s3(p, r):
        own, r_p, r_m = sums[p][0], sums[p][9], sums[p][10]
        total = pair_sum(p, r, y, 0, CH)
        arrived((p, r, 2), own.at[pl.ds(0, 2), rows(r)], to_yp)
        total = total + (r_p[r].astype(F32) + r_m[r].astype(F32))
        if p == 0:
            mg[me, rows(r), :] = (xg[me, rows(r), :].astype(F32) + total).astype(BF16)
            return
        mixed = mg[me, rows(r), :]
        mixed = jnp.where(column[p] == 0, mixed[:, :128], mixed[:, 128:]).astype(F32)
        outv[p - 1, rows(r), :] = (mixed + total).astype(BF16)
        columns = pl.ds(pl.multiple_of(column[p] * 128, 128), 128)
        pltpu.make_async_copy(
            outv.at[p - 1, rows(r)], out.at[rows(r), columns], local_sem.at[5]
        ).start()

    def norm(src, gain, r):
        def body(i, carry):
            at = pl.ds(pl.multiple_of(r * CH + i * 64, 64), 64)
            square = jnp.zeros((64, DV), F32)
            for b in range(8):
                v = src[b, at, :].astype(F32)
                square = square + v * v
            mean = jnp.sum(square, axis=-1, keepdims=True) * (1.0 / D)
            scale = lax.rsqrt(mean + EPS)
            for b in range(8):
                v = src[b, at, :].astype(F32)
                g = gain[pl.ds(b * DV, DV)].reshape(1, DV).astype(F32)
                nrm[at, b * DV : (b + 1) * DV] = (v * scale * g).astype(BF16)
            return carry

        lax.fori_loop(0, CH // 64, body, 0, unroll=2)

    def decays():
        rt = rate[0]
        i = lax.broadcasted_iota(jnp.int32, (CH, CH), 0)
        j = lax.broadcasted_iota(jnp.int32, (CH, CH), 1)
        near = (i - j).astype(F32)
        for d in range(NCH):
            dist = near + float(d * CH)
            value = jnp.exp(-rt * jnp.maximum(dist, 0.0)) * DK ** (-0.5)
            dec[d] = jnp.where(dist >= 0.0, value, 0.0)

    def dot(a, b):
        return jnp.dot(a, b, preferred_element_type=F32)

    def mixa(r):
        a = nrm[rows(r), :]
        qkv = dot(a, wq[:, :, :, 0 : 2 * DK + DV].reshape(D, 2 * DK + DV))
        q = qkv[:, :DK].astype(BF16)
        kbuf[rows(r), :] = qkv[:, DK : 2 * DK].astype(BF16)
        vbuf[rows(r), :] = qkv[:, 2 * DK :].astype(BF16)
        gate = dot(a, wq[:, :, :, 2 * DK + DV :].reshape(D, DV))
        kept = jnp.zeros((CH, DV), F32)
        for b in range(r + 1):
            score = lax.dot_general(
                q, kbuf[rows(b), :], (((1,), (1,)), ((), ())), preferred_element_type=F32
            )
            score = (score * dec[r - b]).astype(BF16)
            kept = kept + dot(score, vbuf[rows(b), :])
        mean = jnp.mean(kept * kept, axis=-1, keepdims=True)
        kept = kept * lax.rsqrt(mean + EPS)
        hid[rows(r), :] = (gate / (1.0 + jnp.exp(-gate)) * kept).astype(BF16)

    def mix(r):
        own, snd = sums[0][:2]
        for b in range(4):
            for dst, cc in ((snd, other), (own, c)):
                right = jnp.concatenate([wo[b, 2 * cc], wo[b, 2 * cc + 1]], axis=1)
                dst[b, rows(r), :] = dot(hid[rows(r), :], right).astype(BF16)

    def up(r):
        a = nrm[rows(r), :]
        for b in range(4):
            upward = dot(a, wu[:, :, :, b * 256 : (b + 1) * 256].reshape(D, 256))
            upward = jnp.maximum(upward, 0.0)
            act[rows(r), b * 256 : (b + 1) * 256] = (upward * upward).astype(BF16)

    def down(p, r):
        own, snd = sums[p][:2]
        for b in (0, 2):
            for dst, cc in ((snd, other), (own, c)):
                at = 2 * cc + column[p]
                right = jnp.concatenate([wd[b, at], wd[b + 1, at]], axis=1)
                value = dot(act[rows(r), :], right).astype(BF16)
                dst[b, rows(r), :] = value[:, :128]
                dst[b + 1, rows(r), :] = value[:, 128:]

    def load(names):
        for i, ref in enumerate((xg.at[me], wq_own, wo.at[zl, x], wu.at[zl, x], wd.at[zl, x])):
            if "tqoud"[i] in names:
                pltpu.make_async_copy(ref, ref, local_sem.at[i]).wait()

    feats = {"t": (xg, gmix), "m": (mg, gmlp)}
    kinds = {"w3": w3, "w4": w4, "w5": w5}
    plain = {
        "load": load, "w1": w1, "w2": w2, "s0": s0, "s1": s1, "s2": s2, "s3": s3,
        "mixa": mixa, "mix": mix, "up": up, "down": down, "decays": decays,
    }
    gathers = {"g1": g1, "g2": g2, "g3": g3, "g4": g4}
    for name, *args in ORDER:
        if name == "norm":
            norm(*feats[args[0]], args[1])
        elif name in gathers:
            gathers[name](args[0], feats[args[0]][0], args[1])
        elif name in plain:
            plain[name](*args)
        else:
            kinds[name[:2]](name[2], *args)
    def left(out_group, whole):
        remote(out_group, next(iter(arrivals)), whole, whole, to_pair).wait_send()

    for w, (buf, _) in weights.items():
        left((w, "first"), shards(w, 3))
        left((w, "third"), buf.at[pl.ds(0, 2)])
        left((w, "fourth"), shards(w, 4))
    for tag, (buf, _) in feats.items():
        left(tag, buf.at[pl.ds(0, 7)])
    for p in range(3):
        own = sums[p][0]
        left(("pair", p), own)
        left(("ring", p), own.at[pl.ds(0, 3)])
    pltpu.make_async_copy(outv, outv, local_sem.at[5]).wait()


def local(
    tokens, gain_mix, query_weight, key_weight, value_weight, gate_weight,
    decay_rate, out_weight, gain_mlp, up_weight, down_weight,
):
    hbm = pl.BlockSpec(memory_space=pltpu.HBM)
    vmem = pl.BlockSpec(memory_space=pltpu.VMEM)
    smem = pl.BlockSpec(memory_space=pltpu.SMEM)

    def summing(width):
        whole = [pltpu.VMEM((4, SEQ, width), BF16)] * 3
        moved = [pltpu.VMEM((NCH, n, width), BF16) for n in (HC, HC, CH, CH)]
        return whole + moved + moved

    return pl.pallas_call(
        kernel,
        out_shape=jax.ShapeDtypeStruct((SEQ, DV), BF16),
        in_specs=[hbm, vmem, hbm, hbm, hbm, hbm, smem, hbm, vmem, hbm, hbm],
        out_specs=hbm,
        scratch_shapes=[
            pltpu.VMEM((8, SEQ, DV), BF16),
            pltpu.VMEM((8, SEQ, DV), BF16),
            pltpu.VMEM((SEQ, D), BF16),
            pltpu.VMEM((4, 4, 128, 768), BF16),
            pltpu.VMEM((4, 4, 256, 128), BF16),
            pltpu.VMEM((4, 4, 128, 1024), BF16),
            pltpu.VMEM((4, 4, 1024, 128), BF16),
            pltpu.VMEM((SEQ, DK), BF16),
            pltpu.VMEM((SEQ, DV), BF16),
            pltpu.VMEM((NCH, CH, CH), F32),
            pltpu.VMEM((SEQ, DV), BF16),
            pltpu.VMEM((SEQ, 1024), BF16),
            pltpu.VMEM((2, SEQ, 128), BF16),
            pltpu.SemaphoreType.DMA((N_SENDS,)),
            pltpu.SemaphoreType.DMA((N_ARRIVALS,)),
            pltpu.SemaphoreType.DMA((N_LOCAL,)),
            *summing(DV), *summing(128), *summing(128),
        ],
        compiler_params=pltpu.CompilerParams(
            collective_id=0, has_side_effects=True, vmem_limit_bytes=62 * 1024 * 1024
        ),
    )(
        tokens, gain_mix, query_weight, key_weight, value_weight, gate_weight,
        decay_rate, out_weight, gain_mlp, up_weight, down_weight,
    )


def solution(mesh):
    finer = Mesh(
        mesh.devices.reshape(mesh.shape["rep"], 4, 4, 4, 2), ("rep", "zl", "x", "y", "c")
    )
    placed = (
        P(("rep", "zl", "x"), TP), P(), P(FS, TP), P(FS, TP), P(FS, TP), P(FS, TP),
        P(TP), P(TP, FS), P(), P(FS, TP), P(TP, FS),
    )
    return jax.shard_map(
        local, mesh=finer, in_specs=placed, out_specs=P(("rep", "zl", "x"), TP), check_vma=False
    )
```

time: 98.3 us -> 93.9 us (0.955)
  Pallas kernels: 95.7 us -> 91.3 us
    pallas_call x1, Pallas kernels: 95.7 us -> 91.3 us  [local(): pl.pallas_call(kernel, out_shape=jax.ShapeDtypeStruct((SEQ, DV), BF16), i...]
where the time goes in v3:
time: 93.9 us; the launch traced here: 93.7 us
  Pallas kernels  91.3 us (97%)
  local copies, waits for them, and re-layouts  1.77 us (2%)
    pallas_call x1, Pallas kernels, local(): pl.pallas_call(kernel, out_shape=jax.ShapeDtypeStruct((SEQ, DV), BF16), i...  91.3 us

profile of v3, /device:TPU:1, one launch (start us, length us, event | category | flops | bytes accessed | tf_op | source)
XLA Modules:
  0.0 93.7 jit_solution(138352117250300082)
XLA Ops:
  0.7 91.3 %shard_map.109 = bf16[768,256]{1,0:T(8,128)(2,1)} custom-call(bf16[768,256]{1,0:T(8,128)(2,1)} %tok.1, bf16[2048]{0:T(1024)(128)(2,1)} %gmix.1, bf16[128,128]{1,0:T(8,128)(2,1)} %qw.1, bf16[128,128]{1,0:T(8,128)(2,1)} %kw.1, bf16[128,256]{1,0:T(8,128)(2,1)} %vw.1, bf16[128,256]{1,0:T(8,128)(2,1)} %gw.1, f32[1]{0:T(128)S(6)} %copy.13.rate, ...), custom_call_target="tpu_custom_call" | custom-call | tf_op jit(solution)/shard_map/pallas_call | solution.py:406
  91.9 1.8 %copy.14 = bf16[768,256]{1,0:T(8,128)(2,1)} copy(bf16[768,256]{1,0:T(8,128)(2,1)} %shard_map.109) | data formatting | bytes 786432

commit v4 on v3

--- a/solution.py
+++ b/solution.py
@@ -27,8 +27,8 @@
     ('w2', 'q', 'A'), ('w2', 'o', 'B'), ('w2', 'o', 'A'), ('w2', 'q', 'B'), ('w3n', 'q', 'A'),
     ('w3n', 'o', 'A'), ('w3n', 'q', 'B'), ('g2', 't', 1), ('w3f', 'o', 'A'), ('w3f', 'q', 'A'),
     ('g3', 't', 1), ('w4o', 'q', 'A'), ('w4o', 'o', 'B'), ('w4o', 'o', 'A'), ('w3f', 'q', 'B'),
-    ('w3f', 'o', 'B'), ('w3n', 'o', 'B'), ('decays',), ('g2', 't', 0), ('g4', 't', 1), ('w4n', 'q', 'A'),
-    ('w4o', 'q', 'B'), ('g2', 't', 2), ('w4n', 'q', 'B'), ('norm', 't', 1), ('w4f', 'q', 'B'),
+    ('w3f', 'o', 'B'), ('w3n', 'o', 'B'), ('g2', 't', 0), ('g4', 't', 1), ('w4n', 'q', 'A'),
+    ('w4o', 'q', 'B'), ('g2', 't', 2), ('w4n', 'q', 'B'), ('load', 'a'), ('norm', 't', 1), ('w4f', 'q', 'B'),
     ('w4f', 'q', 'A'), ('w4n', 'o', 'B'), ('w5o', 'o', 'A'), ('w4n', 'o', 'A'), ('g3', 't', 0),
     ('w4f', 'o', 'A'), ('g3', 't', 2), ('w4f', 'o', 'B'), ('g4', 't', 2), ('w3o', 'u', 'B'), ('w2', 'u', 'B'),
     ('g4', 't', 0), ('w5o', 'q', 'A'), ('w1', 'd', 'B'), ('w5n', 'q', 'B'), ('norm', 't', 2),
@@ -42,26 +42,27 @@
     ('w4f', 'u', 'A'), ('w5o', 'u', 'B'), ('w4o', 'u', 'A'), ('s3', 0, 2), ('g1', 'm', 2), ('w4n', 'u', 'B'),
     ('w3o', 'd', 'A'), ('s3', 0, 1), ('g2', 'm', 0), ('g1', 'm', 1), ('w3f', 'd', 'B'), ('w3o', 'd', 'B'),
     ('g2', 'm', 2), ('w4n', 'd', 'A'), ('w5n', 'u', 'A'), ('w5f', 'u', 'A'), ('w3f', 'd', 'A'),
-    ('g3', 'm', 0), ('g2', 'm', 1), ('w5n', 'u', 'B'), ('g4', 'm', 0), ('norm', 'm', 0), ('w4n', 'd', 'B'),
-    ('w5f', 'u', 'B'), ('w5o', 'u', 'A'), ('g3', 'm', 2), ('up', 0), ('w4f', 'd', 'B'), ('w4o', 'd', 'A'),
-    ('g4', 'm', 2), ('norm', 'm', 2), ('up', 2), ('g3', 'm', 1), ('w5n', 'd', 'A'), ('w4o', 'd', 'B'),
-    ('down', 1, 2), ('s0', 1, 2), ('down', 1, 0), ('s0', 1, 0), ('g4', 'm', 1), ('s1', 1, 2),
-    ('norm', 'm', 1), ('w4f', 'd', 'A'), ('s1', 1, 0), ('up', 1), ('down', 1, 1), ('w5f', 'd', 'B'),
-    ('s0', 1, 1), ('s2', 1, 2), ('s1', 1, 1), ('w5o', 'd', 'A'), ('w5n', 'd', 'B'), ('w5o', 'd', 'B'),
-    ('s2', 1, 0), ('w5f', 'd', 'A'), ('down', 2, 2), ('s0', 2, 2), ('down', 2, 1), ('s0', 2, 1), ('s1', 2, 2),
-    ('down', 2, 0), ('s1', 2, 1), ('s3', 1, 2), ('s0', 2, 0), ('s2', 1, 1), ('s1', 2, 0), ('s2', 2, 2),
-    ('s3', 1, 0), ('s2', 2, 1), ('s3', 1, 1), ('s2', 2, 0), ('s3', 2, 1), ('s3', 2, 2), ('s3', 2, 0),
+    ('g3', 'm', 0), ('g2', 'm', 1), ('w5n', 'u', 'B'), ('g4', 'm', 0), ('load', 'b'), ('norm', 'm', 0),
+    ('w4n', 'd', 'B'), ('w5f', 'u', 'B'), ('w5o', 'u', 'A'), ('g3', 'm', 2), ('up', 0), ('w4f', 'd', 'B'),
+    ('w4o', 'd', 'A'), ('g4', 'm', 2), ('norm', 'm', 2), ('up', 2), ('g3', 'm', 1), ('w5n', 'd', 'A'),
+    ('w4o', 'd', 'B'), ('down', 1, 2), ('s0', 1, 2), ('down', 1, 0), ('s0', 1, 0), ('g4', 'm', 1),
+    ('s1', 1, 2), ('norm', 'm', 1), ('w4f', 'd', 'A'), ('s1', 1, 0), ('up', 1), ('down', 1, 1),
+    ('w5f', 'd', 'B'), ('s0', 1, 1), ('s2', 1, 2), ('s1', 1, 1), ('w5o', 'd', 'A'), ('w5n', 'd', 'B'),
+    ('w5o', 'd', 'B'), ('s2', 1, 0), ('w5f', 'd', 'A'), ('down', 2, 2), ('s0', 2, 2), ('down', 2, 1),
+    ('s0', 2, 1), ('s1', 2, 2), ('down', 2, 0), ('s1', 2, 1), ('s3', 1, 2), ('s0', 2, 0), ('s2', 1, 1),
+    ('s1', 2, 0), ('s2', 2, 2), ('s3', 1, 0), ('s2', 2, 1), ('s3', 1, 1), ('s2', 2, 0), ('s3', 2, 1),
+    ('s3', 2, 2), ('s3', 2, 0),
 ]
 MESH_ID = pl.DeviceIdType.MESH
 N_SENDS = 20
 N_ARRIVALS = 97
-N_LOCAL = 6
+N_LOCAL = 7
 
 
 def kernel(
-    tok, gmix, qw, kw, vw, gw, rate, ow, gmlp, uw, dw,
+    tok, gain_mix, qw, kw, vw, gw, rate, ow, gain_mlp, uw, dw,
     out,
-    xg, mg, nrm, wq, wo, wu, wd, kbuf, vbuf, dec, hid, act, outv,
+    gmix, gmlp, xg, mg, nrm, wq, wo, wu, wd, kbuf, vbuf, dec, hid, act,
     send_sem, recv_sem, local_sem, *summing,
 ):
     sums = [summing[11 * p : 11 * p + 11] for p in range(3)]
@@ -114,10 +115,23 @@
         (2, ow, wo.at[zl, x]),
         (3, uw, wu.at[zl, x]),
         (4, dw, wd.at[zl, x]),
+        (5, gain_mix, gmix),
+        (6, gain_mlp, gmlp),
     ]
     for i, src, dst in loads:
         pltpu.make_async_copy(src, dst, local_sem.at[i]).start()
 
+    def decays():
+        rt = rate[0]
+        i = lax.broadcasted_iota(jnp.int32, (CH, CH), 0)
+        j = lax.broadcasted_iota(jnp.int32, (CH, CH), 1)
+        near = (i - j).astype(F32)
+        for d in range(NCH):
+            dist = near + float(d * CH)
+            value = jnp.exp(-rt * jnp.maximum(dist, 0.0)) * DK ** (-0.5)
+            dec[d] = jnp.where(dist >= 0.0, value, 0.0)
+
+    decays()
     barrier = pltpu.get_barrier_semaphore()
     for dev in (to_xp, to_xm, to_zp, to_zm, to_yp, to_ym, to_pair):
         pl.semaphore_signal(barrier, inc=1, device_id=dev, device_id_type=MESH_ID)
@@ -275,11 +289,8 @@
             return
         mixed = mg[me, rows(r), :]
         mixed = jnp.where(column[p] == 0, mixed[:, :128], mixed[:, 128:]).astype(F32)
-        outv[p - 1, rows(r), :] = (mixed + total).astype(BF16)
         columns = pl.ds(pl.multiple_of(column[p] * 128, 128), 128)
-        pltpu.make_async_copy(
-            outv.at[p - 1, rows(r)], out.at[rows(r), columns], local_sem.at[5]
-        ).start()
+        out[rows(r), columns] = (mixed + total).astype(BF16)
 
     def norm(src, gain, r):
         def body(i, carry):
@@ -297,16 +308,6 @@
             return carry
 
         lax.fori_loop(0, CH // 64, body, 0, unroll=2)
-
-    def decays():
-        rt = rate[0]
-        i = lax.broadcasted_iota(jnp.int32, (CH, CH), 0)
-        j = lax.broadcasted_iota(jnp.int32, (CH, CH), 1)
-        near = (i - j).astype(F32)
-        for d in range(NCH):
-            dist = near + float(d * CH)
-            value = jnp.exp(-rt * jnp.maximum(dist, 0.0)) * DK ** (-0.5)
-            dec[d] = jnp.where(dist >= 0.0, value, 0.0)
 
     def dot(a, b):
         return jnp.dot(a, b, preferred_element_type=F32)
@@ -354,15 +355,16 @@
                 dst[b + 1, rows(r), :] = value[:, 128:]
 
     def load(names):
-        for i, ref in enumerate((xg.at[me], wq_own, wo.at[zl, x], wu.at[zl, x], wd.at[zl, x])):
-            if "tqoud"[i] in names:
+        own = (xg.at[me], wq_own, wo.at[zl, x], wu.at[zl, x], wd.at[zl, x], gmix, gmlp)
+        for i, ref in enumerate(own):
+            if "tqoudab"[i] in names:
                 pltpu.make_async_copy(ref, ref, local_sem.at[i]).wait()
 
     feats = {"t": (xg, gmix), "m": (mg, gmlp)}
     kinds = {"w3": w3, "w4": w4, "w5": w5}
     plain = {
         "load": load, "w1": w1, "w2": w2, "s0": s0, "s1": s1, "s2": s2, "s3": s3,
-        "mixa": mixa, "mix": mix, "up": up, "down": down, "decays": decays,
+        "mixa": mixa, "mix": mix, "up": up, "down": down,
     }
     gathers = {"g1": g1, "g2": g2, "g3": g3, "g4": g4}
     for name, *args in ORDER:
@@ -387,7 +389,6 @@
         own = sums[p][0]
         left(("pair", p), own)
         left(("ring", p), own.at[pl.ds(0, 3)])
-    pltpu.make_async_copy(outv, outv, local_sem.at[5]).wait()
 
 
 def local(
@@ -403,12 +404,17 @@
         moved = [pltpu.VMEM((NCH, n, width), BF16) for n in (HC, HC, CH, CH)]
         return whole + moved + moved
 
+    def stay(v):
+        return pltpu.with_memory_space_constraint(v, pltpu.HBM)
+
     return pl.pallas_call(
         kernel,
         out_shape=jax.ShapeDtypeStruct((SEQ, DV), BF16),
-        in_specs=[hbm, vmem, hbm, hbm, hbm, hbm, smem, hbm, vmem, hbm, hbm],
-        out_specs=hbm,
+        in_specs=[hbm, hbm, hbm, hbm, hbm, hbm, smem, hbm, hbm, hbm, hbm],
+        out_specs=vmem,
         scratch_shapes=[
+            pltpu.VMEM((D,), BF16),
+            pltpu.VMEM((D,), BF16),
             pltpu.VMEM((8, SEQ, DV), BF16),
             pltpu.VMEM((8, SEQ, DV), BF16),
             pltpu.VMEM((SEQ, D), BF16),
@@ -421,18 +427,18 @@
             pltpu.VMEM((NCH, CH, CH), F32),
             pltpu.VMEM((SEQ, DV), BF16),
             pltpu.VMEM((SEQ, 1024), BF16),
-            pltpu.VMEM((2, SEQ, 128), BF16),
             pltpu.SemaphoreType.DMA((N_SENDS,)),
             pltpu.SemaphoreType.DMA((N_ARRIVALS,)),
             pltpu.SemaphoreType.DMA((N_LOCAL,)),
             *summing(DV), *summing(128), *summing(128),
         ],
         compiler_params=pltpu.CompilerParams(
-            collective_id=0, has_side_effects=True, vmem_limit_bytes=62 * 1024 * 1024
+            collective_id=0, has_side_effects=True, vmem_limit_bytes=52 * 1024 * 1024
         ),
     )(
-        tokens, gain_mix, query_weight, key_weight, value_weight, gate_weight,
-        decay_rate, out_weight, gain_mlp, up_weight, down_weight,
+        stay(tokens), stay(gain_mix), stay(query_weight), stay(key_weight), stay(value_weight),
+        stay(gate_weight), decay_rate, stay(out_weight), stay(gain_mlp), stay(up_weight),
+        stay(down_weight),
     )
 
 

time: 93.9 us -> 91.7 us (0.977)
  Pallas kernels: 91.3 us -> 90.2 us
  local copies, waits for them, and re-layouts: 1.77 us -> 0.75 us
    pallas_call x1, Pallas kernels: 91.3 us -> 90.2 us  [local(): pl.pallas_call(kernel, out_shape=jax.ShapeDtypeStruct((SEQ, DV), BF16), i...]
    unnamed x1, local copies, waits for them, and re-layouts: 1.77 us -> 0.75 us
where the time goes in v4:
time: 91.7 us; the launch traced here: 91.6 us
  Pallas kernels  90.2 us (98%)
    pallas_call x1, Pallas kernels, local(): pl.pallas_call(kernel, out_shape=jax.ShapeDtypeStruct((SEQ, DV), BF16), i...  90.2 us

profile of v4, /device:TPU:1, one launch (start us, length us, event | category | flops | bytes accessed | tf_op | source)
XLA Modules:
  0.0 91.6 jit_solution(2895290673052024063)
XLA Ops:
  0.7 90.2 %shard_map.109 = bf16[768,256]{1,0:T(8,128)(2,1)S(1)} custom-call(bf16[768,256]{1,0:T(8,128)(2,1)} %tok.1, bf16[2048]{0:T(1024)(128)(2,1)} %gain_mix.1, bf16[128,128]{1,0:T(8,128)(2,1)} %qw.1, bf16[128,128]{1,0:T(8,128)(2,1)} %kw.1, bf16[128,256]{1,0:T(8,128)(2,1)} %vw.1, bf16[128,256]{1,0:T(8,128)(2,1)} %gw.1, f32[1]{0:T(128)S(6)} %copy.13.rate, ...), custom_call_target="tpu_custom_call" | custom-call | tf_op jit(solution)/shard_map/pallas_call | solution.py:410
  90.9 0.7 copy.14

commit v5 on v4

--- a/solution.py
+++ b/solution.py
@@ -25,33 +25,32 @@
     ('load', 'o'), ('w1', 'o', 'B'), ('w3o', 'o', 'A'), ('g1', 't', 2), ('w1', 'o', 'A'), ('w3o', 'q', 'B'),
     ('w3o', 'q', 'A'), ('w1', 'u', 'A'), ('g1', 't', 0), ('w3o', 'o', 'B'), ('w1', 'u', 'B'),
     ('w2', 'q', 'A'), ('w2', 'o', 'B'), ('w2', 'o', 'A'), ('w2', 'q', 'B'), ('w3n', 'q', 'A'),
-    ('w3n', 'o', 'A'), ('w3n', 'q', 'B'), ('g2', 't', 1), ('w3f', 'o', 'A'), ('w3f', 'q', 'A'),
-    ('g3', 't', 1), ('w4o', 'q', 'A'), ('w4o', 'o', 'B'), ('w4o', 'o', 'A'), ('w3f', 'q', 'B'),
-    ('w3f', 'o', 'B'), ('w3n', 'o', 'B'), ('g2', 't', 0), ('g4', 't', 1), ('w4n', 'q', 'A'),
-    ('w4o', 'q', 'B'), ('g2', 't', 2), ('w4n', 'q', 'B'), ('load', 'a'), ('norm', 't', 1), ('w4f', 'q', 'B'),
-    ('w4f', 'q', 'A'), ('w4n', 'o', 'B'), ('w5o', 'o', 'A'), ('w4n', 'o', 'A'), ('g3', 't', 0),
-    ('w4f', 'o', 'A'), ('g3', 't', 2), ('w4f', 'o', 'B'), ('g4', 't', 2), ('w3o', 'u', 'B'), ('w2', 'u', 'B'),
-    ('g4', 't', 0), ('w5o', 'q', 'A'), ('w1', 'd', 'B'), ('w5n', 'q', 'B'), ('norm', 't', 2),
-    ('norm', 't', 0), ('w5f', 'q', 'B'), ('w2', 'u', 'A'), ('w5f', 'q', 'A'), ('w5n', 'q', 'A'),
-    ('w5o', 'o', 'B'), ('w3o', 'u', 'A'), ('w5o', 'q', 'B'), ('w1', 'd', 'A'), ('mixa', 0), ('w5n', 'o', 'A'),
-    ('w5n', 'o', 'B'), ('w5f', 'o', 'A'), ('w5f', 'o', 'B'), ('mix', 0), ('s0', 0, 0), ('mixa', 1),
-    ('w3n', 'u', 'A'), ('mix', 1), ('s0', 0, 1), ('s1', 0, 0), ('w3f', 'u', 'B'), ('mixa', 2), ('mix', 2),
-    ('s0', 0, 2), ('s1', 0, 1), ('w3n', 'u', 'B'), ('s1', 0, 2), ('w2', 'd', 'A'), ('s2', 0, 0),
-    ('w2', 'd', 'B'), ('s2', 0, 1), ('w4o', 'u', 'B'), ('w3f', 'u', 'A'), ('s2', 0, 2), ('s3', 0, 0),
-    ('g1', 'm', 0), ('w4n', 'u', 'A'), ('w3n', 'd', 'A'), ('w3n', 'd', 'B'), ('w4f', 'u', 'B'),
-    ('w4f', 'u', 'A'), ('w5o', 'u', 'B'), ('w4o', 'u', 'A'), ('s3', 0, 2), ('g1', 'm', 2), ('w4n', 'u', 'B'),
-    ('w3o', 'd', 'A'), ('s3', 0, 1), ('g2', 'm', 0), ('g1', 'm', 1), ('w3f', 'd', 'B'), ('w3o', 'd', 'B'),
-    ('g2', 'm', 2), ('w4n', 'd', 'A'), ('w5n', 'u', 'A'), ('w5f', 'u', 'A'), ('w3f', 'd', 'A'),
-    ('g3', 'm', 0), ('g2', 'm', 1), ('w5n', 'u', 'B'), ('g4', 'm', 0), ('load', 'b'), ('norm', 'm', 0),
-    ('w4n', 'd', 'B'), ('w5f', 'u', 'B'), ('w5o', 'u', 'A'), ('g3', 'm', 2), ('up', 0), ('w4f', 'd', 'B'),
-    ('w4o', 'd', 'A'), ('g4', 'm', 2), ('norm', 'm', 2), ('up', 2), ('g3', 'm', 1), ('w5n', 'd', 'A'),
-    ('w4o', 'd', 'B'), ('down', 1, 2), ('s0', 1, 2), ('down', 1, 0), ('s0', 1, 0), ('g4', 'm', 1),
-    ('s1', 1, 2), ('norm', 'm', 1), ('w4f', 'd', 'A'), ('s1', 1, 0), ('up', 1), ('down', 1, 1),
-    ('w5f', 'd', 'B'), ('s0', 1, 1), ('s2', 1, 2), ('s1', 1, 1), ('w5o', 'd', 'A'), ('w5n', 'd', 'B'),
-    ('w5o', 'd', 'B'), ('s2', 1, 0), ('w5f', 'd', 'A'), ('down', 2, 2), ('s0', 2, 2), ('down', 2, 1),
-    ('s0', 2, 1), ('s1', 2, 2), ('down', 2, 0), ('s1', 2, 1), ('s3', 1, 2), ('s0', 2, 0), ('s2', 1, 1),
-    ('s1', 2, 0), ('s2', 2, 2), ('s3', 1, 0), ('s2', 2, 1), ('s3', 1, 1), ('s2', 2, 0), ('s3', 2, 1),
-    ('s3', 2, 2), ('s3', 2, 0),
+    ('w3n', 'o', 'A'), ('w3n', 'q', 'B'), ('g2', 't', 1), ('g2', 't', 2), ('g2', 't', 0), ('w3f', 'o', 'A'),
+    ('w3f', 'q', 'A'), ('g3', 't', 1), ('w4o', 'q', 'A'), ('w4o', 'o', 'B'), ('w4o', 'o', 'A'),
+    ('w3f', 'q', 'B'), ('w3f', 'o', 'B'), ('w3n', 'o', 'B'), ('g4', 't', 1), ('w4n', 'q', 'A'),
+    ('w4o', 'q', 'B'), ('w4n', 'q', 'B'), ('g3', 't', 2), ('g3', 't', 0), ('load', 'a'), ('norm', 't', 1),
+    ('w4f', 'q', 'B'), ('g4', 't', 2), ('g4', 't', 0), ('norm', 't', 0), ('norm', 't', 2), ('w4f', 'q', 'A'),
+    ('w4n', 'o', 'B'), ('w5o', 'o', 'A'), ('w4n', 'o', 'A'), ('w4f', 'o', 'A'), ('w4f', 'o', 'B'),
+    ('w3o', 'u', 'B'), ('w2', 'u', 'B'), ('w5o', 'q', 'A'), ('w1', 'd', 'B'), ('w5n', 'q', 'B'),
+    ('w5f', 'q', 'B'), ('w2', 'u', 'A'), ('w5f', 'q', 'A'), ('w5n', 'q', 'A'), ('w5o', 'o', 'B'),
+    ('w3o', 'u', 'A'), ('w5o', 'q', 'B'), ('w1', 'd', 'A'), ('mixa', 0), ('w5n', 'o', 'A'), ('w5n', 'o', 'B'),
+    ('w5f', 'o', 'A'), ('w5f', 'o', 'B'), ('mix', 0), ('s0', 0, 0), ('mixa', 1), ('w3n', 'u', 'A'),
+    ('mix', 1), ('s0', 0, 1), ('s1', 0, 0), ('w3f', 'u', 'B'), ('mixa', 2), ('mix', 2), ('s0', 0, 2),
+    ('s1', 0, 1), ('w3n', 'u', 'B'), ('s1', 0, 2), ('w2', 'd', 'A'), ('s2', 0, 0), ('w2', 'd', 'B'),
+    ('s2', 0, 1), ('w4o', 'u', 'B'), ('w3f', 'u', 'A'), ('s2', 0, 2), ('s3', 0, 0), ('g1', 'm', 0),
+    ('w4n', 'u', 'A'), ('w3n', 'd', 'A'), ('w3n', 'd', 'B'), ('w4f', 'u', 'B'), ('w4f', 'u', 'A'),
+    ('w5o', 'u', 'B'), ('w4o', 'u', 'A'), ('s3', 0, 2), ('g1', 'm', 2), ('w4n', 'u', 'B'), ('w3o', 'd', 'A'),
+    ('s3', 0, 1), ('g2', 'm', 0), ('g1', 'm', 1), ('w3f', 'd', 'B'), ('w3o', 'd', 'B'), ('g2', 'm', 2),
+    ('w4n', 'd', 'A'), ('w5n', 'u', 'A'), ('w5f', 'u', 'A'), ('w3f', 'd', 'A'), ('g3', 'm', 0),
+    ('g2', 'm', 1), ('w5n', 'u', 'B'), ('g4', 'm', 0), ('load', 'b'), ('norm', 'm', 0), ('w4n', 'd', 'B'),
+    ('w5f', 'u', 'B'), ('w5o', 'u', 'A'), ('g3', 'm', 2), ('up', 0), ('w4f', 'd', 'B'), ('w4o', 'd', 'A'),
+    ('g4', 'm', 2), ('norm', 'm', 2), ('up', 2), ('g3', 'm', 1), ('w5n', 'd', 'A'), ('w4o', 'd', 'B'),
+    ('down', 1, 2), ('s0', 1, 2), ('down', 1, 0), ('s0', 1, 0), ('g4', 'm', 1), ('s1', 1, 2),
+    ('norm', 'm', 1), ('w4f', 'd', 'A'), ('s1', 1, 0), ('up', 1), ('down', 1, 1), ('w5f', 'd', 'B'),
+    ('s0', 1, 1), ('s2', 1, 2), ('s1', 1, 1), ('w5o', 'd', 'A'), ('w5n', 'd', 'B'), ('w5o', 'd', 'B'),
+    ('s2', 1, 0), ('w5f', 'd', 'A'), ('down', 2, 2), ('s0', 2, 2), ('down', 2, 1), ('s0', 2, 1), ('s1', 2, 2),
+    ('down', 2, 0), ('s1', 2, 1), ('s3', 1, 2), ('s0', 2, 0), ('s2', 1, 1), ('s1', 2, 0), ('s2', 2, 2),
+    ('s3', 1, 0), ('s2', 2, 1), ('s3', 1, 1), ('s2', 2, 0), ('s3', 2, 1), ('s3', 2, 2), ('s3', 2, 0),
 ]
 MESH_ID = pl.DeviceIdType.MESH
 N_SENDS = 20

time: 91.7 us -> 91.5 us (level)
  no operation moved by 1% of the time
where the time goes in v5:
time: 91.5 us; the launch traced here: 91.4 us
  Pallas kernels  90 us (98%)
    pallas_call x1, Pallas kernels, local(): pl.pallas_call(kernel, out_shape=jax.ShapeDtypeStruct((SEQ, DV), BF16), i...  90 us

profile of v5, /device:TPU:1, one launch (start us, length us, event | category | flops | bytes accessed | tf_op | source)
XLA Modules:
  0.0 91.4 jit_solution(12507370093431573277)
XLA Ops:
  0.7 90.0 %shard_map.109 = bf16[768,256]{1,0:T(8,128)(2,1)S(1)} custom-call(bf16[768,256]{1,0:T(8,128)(2,1)} %tok.1, bf16[2048]{0:T(1024)(128)(2,1)} %gain_mix.1, bf16[128,128]{1,0:T(8,128)(2,1)} %qw.1, bf16[128,128]{1,0:T(8,128)(2,1)} %kw.1, bf16[128,256]{1,0:T(8,128)(2,1)} %vw.1, bf16[128,256]{1,0:T(8,128)(2,1)} %gw.1, f32[1]{0:T(128)S(6)} %copy.13.rate, ...), custom_call_target="tpu_custom_call" | custom-call | tf_op jit(solution)/shard_map/pallas_call | solution.py:409
  90.6 0.7 copy.14

commit v6 on v5

--- a/solution.py
+++ b/solution.py
@@ -34,23 +34,22 @@
     ('w3o', 'u', 'B'), ('w2', 'u', 'B'), ('w5o', 'q', 'A'), ('w1', 'd', 'B'), ('w5n', 'q', 'B'),
     ('w5f', 'q', 'B'), ('w2', 'u', 'A'), ('w5f', 'q', 'A'), ('w5n', 'q', 'A'), ('w5o', 'o', 'B'),
     ('w3o', 'u', 'A'), ('w5o', 'q', 'B'), ('w1', 'd', 'A'), ('mixa', 0), ('w5n', 'o', 'A'), ('w5n', 'o', 'B'),
-    ('w5f', 'o', 'A'), ('w5f', 'o', 'B'), ('mix', 0), ('s0', 0, 0), ('mixa', 1), ('w3n', 'u', 'A'),
-    ('mix', 1), ('s0', 0, 1), ('s1', 0, 0), ('w3f', 'u', 'B'), ('mixa', 2), ('mix', 2), ('s0', 0, 2),
-    ('s1', 0, 1), ('w3n', 'u', 'B'), ('s1', 0, 2), ('w2', 'd', 'A'), ('s2', 0, 0), ('w2', 'd', 'B'),
-    ('s2', 0, 1), ('w4o', 'u', 'B'), ('w3f', 'u', 'A'), ('s2', 0, 2), ('s3', 0, 0), ('g1', 'm', 0),
-    ('w4n', 'u', 'A'), ('w3n', 'd', 'A'), ('w3n', 'd', 'B'), ('w4f', 'u', 'B'), ('w4f', 'u', 'A'),
-    ('w5o', 'u', 'B'), ('w4o', 'u', 'A'), ('s3', 0, 2), ('g1', 'm', 2), ('w4n', 'u', 'B'), ('w3o', 'd', 'A'),
-    ('s3', 0, 1), ('g2', 'm', 0), ('g1', 'm', 1), ('w3f', 'd', 'B'), ('w3o', 'd', 'B'), ('g2', 'm', 2),
-    ('w4n', 'd', 'A'), ('w5n', 'u', 'A'), ('w5f', 'u', 'A'), ('w3f', 'd', 'A'), ('g3', 'm', 0),
-    ('g2', 'm', 1), ('w5n', 'u', 'B'), ('g4', 'm', 0), ('load', 'b'), ('norm', 'm', 0), ('w4n', 'd', 'B'),
-    ('w5f', 'u', 'B'), ('w5o', 'u', 'A'), ('g3', 'm', 2), ('up', 0), ('w4f', 'd', 'B'), ('w4o', 'd', 'A'),
-    ('g4', 'm', 2), ('norm', 'm', 2), ('up', 2), ('g3', 'm', 1), ('w5n', 'd', 'A'), ('w4o', 'd', 'B'),
-    ('down', 1, 2), ('s0', 1, 2), ('down', 1, 0), ('s0', 1, 0), ('g4', 'm', 1), ('s1', 1, 2),
+    ('w5f', 'o', 'A'), ('w5f', 'o', 'B'), ('mix', 0), ('mixa', 1), ('w3n', 'u', 'A'), ('mix', 1),
+    ('s1', 0, 0), ('w3f', 'u', 'B'), ('mixa', 2), ('mix', 2), ('s1', 0, 1), ('w3n', 'u', 'B'), ('s1', 0, 2),
+    ('w2', 'd', 'A'), ('s2', 0, 0), ('w2', 'd', 'B'), ('s2', 0, 1), ('w4o', 'u', 'B'), ('w3f', 'u', 'A'),
+    ('s2', 0, 2), ('s3', 0, 0), ('g1', 'm', 0), ('w4n', 'u', 'A'), ('w3n', 'd', 'A'), ('w3n', 'd', 'B'),
+    ('w4f', 'u', 'B'), ('w4f', 'u', 'A'), ('w5o', 'u', 'B'), ('w4o', 'u', 'A'), ('s3', 0, 2), ('g1', 'm', 2),
+    ('w4n', 'u', 'B'), ('w3o', 'd', 'A'), ('s3', 0, 1), ('g2', 'm', 0), ('g1', 'm', 1), ('w3f', 'd', 'B'),
+    ('w3o', 'd', 'B'), ('g2', 'm', 2), ('w4n', 'd', 'A'), ('w5n', 'u', 'A'), ('w5f', 'u', 'A'),
+    ('w3f', 'd', 'A'), ('g3', 'm', 0), ('g2', 'm', 1), ('w5n', 'u', 'B'), ('g4', 'm', 0), ('load', 'b'),
+    ('norm', 'm', 0), ('w4n', 'd', 'B'), ('w5f', 'u', 'B'), ('w5o', 'u', 'A'), ('g3', 'm', 2), ('up', 0),
+    ('w4f', 'd', 'B'), ('w4o', 'd', 'A'), ('g4', 'm', 2), ('norm', 'm', 2), ('up', 2), ('g3', 'm', 1),
+    ('w5n', 'd', 'A'), ('w4o', 'd', 'B'), ('down', 1, 2), ('down', 1, 0), ('g4', 'm', 1), ('s1', 1, 2),
     ('norm', 'm', 1), ('w4f', 'd', 'A'), ('s1', 1, 0), ('up', 1), ('down', 1, 1), ('w5f', 'd', 'B'),
-    ('s0', 1, 1), ('s2', 1, 2), ('s1', 1, 1), ('w5o', 'd', 'A'), ('w5n', 'd', 'B'), ('w5o', 'd', 'B'),
-    ('s2', 1, 0), ('w5f', 'd', 'A'), ('down', 2, 2), ('s0', 2, 2), ('down', 2, 1), ('s0', 2, 1), ('s1', 2, 2),
-    ('down', 2, 0), ('s1', 2, 1), ('s3', 1, 2), ('s0', 2, 0), ('s2', 1, 1), ('s1', 2, 0), ('s2', 2, 2),
-    ('s3', 1, 0), ('s2', 2, 1), ('s3', 1, 1), ('s2', 2, 0), ('s3', 2, 1), ('s3', 2, 2), ('s3', 2, 0),
+    ('s2', 1, 2), ('s1', 1, 1), ('w5o', 'd', 'A'), ('w5n', 'd', 'B'), ('w5o', 'd', 'B'), ('s2', 1, 0),
+    ('w5f', 'd', 'A'), ('down', 2, 2), ('down', 2, 1), ('s1', 2, 2), ('down', 2, 0), ('s1', 2, 1),
+    ('s3', 1, 2), ('s2', 1, 1), ('s1', 2, 0), ('s2', 2, 2), ('s3', 1, 0), ('s2', 2, 1), ('s3', 1, 1),
+    ('s2', 2, 0), ('s3', 2, 1), ('s3', 2, 2), ('s3', 2, 0),
 ]
 MESH_ID = pl.DeviceIdType.MESH
 N_SENDS = 20
@@ -331,10 +330,12 @@
 
     def mix(r):
         own, snd = sums[0][:2]
-        for b in range(4):
-            for dst, cc in ((snd, other), (own, c)):
+        for dst, cc in ((snd, other), (own, c)):
+            for b in range(4):
                 right = jnp.concatenate([wo[b, 2 * cc], wo[b, 2 * cc + 1]], axis=1)
                 dst[b, rows(r), :] = dot(hid[rows(r), :], right).astype(BF16)
+            if dst is snd:
+                s0(0, r)
 
     def up(r):
         a = nrm[rows(r), :]
@@ -345,13 +346,15 @@
 
     def down(p, r):
         own, snd = sums[p][:2]
-        for b in (0, 2):
-            for dst, cc in ((snd, other), (own, c)):
+        for dst, cc in ((snd, other), (own, c)):
+            for b in (0, 2):
                 at = 2 * cc + column[p]
                 right = jnp.concatenate([wd[b, at], wd[b + 1, at]], axis=1)
                 value = dot(act[rows(r), :], right).astype(BF16)
                 dst[b, rows(r), :] = value[:, :128]
                 dst[b + 1, rows(r), :] = value[:, 128:]
+            if dst is snd:
+                s0(p, r)
 
     def load(names):
         own = (xg.at[me], wq_own, wo.at[zl, x], wu.at[zl, x], wd.at[zl, x], gmix, gmlp)
@@ -362,7 +365,7 @@
     feats = {"t": (xg, gmix), "m": (mg, gmlp)}
     kinds = {"w3": w3, "w4": w4, "w5": w5}
     plain = {
-        "load": load, "w1": w1, "w2": w2, "s0": s0, "s1": s1, "s2": s2, "s3": s3,
+        "load": load, "w1": w1, "w2": w2, "s1": s1, "s2": s2, "s3": s3,
         "mixa": mixa, "mix": mix, "up": up, "down": down,
     }
     gathers = {"g1": g1, "g2": g2, "g3": g3, "g4": g4}

time: 91.5 us -> 91 us (level)
  no operation moved by 1% of the time
where the time goes in v6:
time: 91 us; the launch traced here: 90.9 us
  Pallas kernels  89.5 us (98%)
    pallas_call x1, Pallas kernels, local(): pl.pallas_call(kernel, out_shape=jax.ShapeDtypeStruct((SEQ, DV), BF16), i...  89.5 us

profile of v6, /device:TPU:1, one launch (start us, length us, event | category | flops | bytes accessed | tf_op | source)
XLA Modules:
  0.0 90.9 jit_solution(5407666628591299044)
XLA Ops:
  0.7 89.5 %shard_map.109 = bf16[768,256]{1,0:T(8,128)(2,1)S(1)} custom-call(bf16[768,256]{1,0:T(8,128)(2,1)} %tok.1, bf16[2048]{0:T(1024)(128)(2,1)} %gain_mix.1, bf16[128,128]{1,0:T(8,128)(2,1)} %qw.1, bf16[128,128]{1,0:T(8,128)(2,1)} %kw.1, bf16[128,256]{1,0:T(8,128)(2,1)} %vw.1, bf16[128,256]{1,0:T(8,128)(2,1)} %gw.1, f32[1]{0:T(128)S(6)} %copy.13.rate, ...), custom_call_target="tpu_custom_call" | custom-call | tf_op jit(solution)/shard_map/pallas_call | solution.py:412
  90.2 0.7 copy.14
